TPU v7x, 512 devices: a whole 4x4x16 slice. The times are simulated.
512 devices in a mesh: rep: 2 (over z_hi), fs: 32 (over z_lo, y), tp: 8 (over x, core).
Axes of the slice: x: 4, y: 4, z: 16 (z_hi: 2, z_lo: 8; z = z_hi * 8 + z_lo), core: 2. Of those that a mesh axis runs over, the one named last changes fastest.
Arguments:
- incoming_features: bfloat16 [12288, 2048], P(('rep', 'fs'), 'tp'), may hold values from -6 to 6
- attend_prenormal_scale: bfloat16 [2048], replicated, may hold values from 0.099609375 to 1.8984375
- probe_matrix: bfloat16 [2048, 512], P('fs', 'tp'), may hold values from -0.125 to 0.125
- lookup_matrix: bfloat16 [2048, 512], P('fs', 'tp'), may hold values from -0.125 to 0.125
- content_matrix: bfloat16 [2048, 1024], P('fs', 'tp'), may hold values from -0.125 to 0.125
- forgetting_matrix: bfloat16 [2048, 512], P('fs', 'tp'), may hold values from -0.125 to 0.125
- result_switch_matrix: bfloat16 [2048, 1024], P('fs', 'tp'), may hold values from -0.125 to 0.125
- forgetting_shift: float32 [512], P('tp'), may hold values from -0.5 to 5.5
- spike_forget_logarithm: float32 [12288, 512], P(('rep', 'fs'), 'tp'), may hold values from -0.7 to 0
- attend_unit_scale: bfloat16 [1024], P('tp'), may hold values from 0.099609375 to 1.8984375
- attend_result_matrix: bfloat16 [1024, 2048], P('tp', 'fs'), may hold values from -0.1875 to 0.1875
- perceptron_scale: bfloat16 [2048], replicated, may hold values from 0.099609375 to 1.8984375
- content_expand_matrix: bfloat16 [2048, 4096], P('fs', 'tp'), may hold values from -0.125 to 0.125
- switch_expand_matrix: bfloat16 [2048, 4096], P('fs', 'tp'), may hold values from -0.125 to 0.125
- content_kernel: bfloat16 [3, 4096], P(None, 'tp'), may hold values from -3.5 to 3.5
- switch_kernel: bfloat16 [3, 4096], P(None, 'tp'), may hold values from -3.5 to 3.5
- contract_matrix: bfloat16 [4096, 2048], P('tp', 'fs'), may hold values from -0.09375 to 0.09375
Outputs:
- out_rows: bfloat16 [12288, 2048], P(('rep', 'fs'), 'tp')
All inputs are finite; a program needn't handle non-finite values.
Results may differ from a plain program's by a relative error of at most 0.02.
Values may be sent and summed in bfloat16 or wider, within the bound.
A program may use at most 64 MiB of HBM per device.

v0:
```python
import jax
import jax.numpy as jnp
from jax import lax
from jax.sharding import PartitionSpec as P

HEAD_K = 32
HEAD_V = 64
BLOCK = 64


norm_eps = 1e-06
switch_multiplier = 16.0


def sent_together(arrays, axis, dim, along):
    both = jnp.concatenate(arrays, axis=along)
    result, at, outs = (lax.all_gather(both, axis, axis=dim, tiled=True), 0, [])
    for a in arrays:
        outs.append(lax.slice_in_dim(result, at, at + a.shape[along], axis=along))
        at += a.shape[along]
    return tuple(outs)


def sent_to_all(array, axis):
    devices = lax.axis_size(axis)
    return lax.all_to_all(
        jnp.broadcast_to(array[None], (devices, *array.shape)), axis, 0, 0, tiled=True
    )


def laid_out(blocks, dim):
    blocks = jnp.moveaxis(blocks, 0, dim)
    dims = blocks.shape
    return blocks.reshape(*dims[:dim], dims[dim] * dims[dim + 1], *dims[dim + 2 :])


def gather_directly(array, axis, dim):
    blocks = sent_to_all(array, axis)
    return laid_out(blocks, dim)


def taken_together(array, axis):
    return sent_to_all(array, axis).astype(jnp.float32).sum(axis=0)


def split_up(array, dim, devices):
    before, after = (array.shape[:dim], array.shape[dim + 1 :])
    return jnp.moveaxis(array.reshape(*before, devices, -1, *after), dim, 0)


def summed_on_arrival(array, axis, dim):
    devices = lax.axis_size(axis)
    blocks = lax.all_to_all(split_up(array, dim, devices), axis, 0, 0, tiled=True)
    return jnp.sum(blocks.astype(jnp.float32), axis=0)


def row_norm(content_tokens, gain):
    content_tokens = content_tokens.astype(jnp.float32)
    scaled = content_tokens * lax.rsqrt(
        jnp.mean(content_tokens * content_tokens, axis=-1, keepdims=True) + norm_eps
    )
    return (scaled * gain.astype(jnp.float32)).astype(jnp.bfloat16)


def gated_scan(probe_tokens, lookup_tokens, content_tokens, forgetting_scores):
    length, heads, key_size = probe_tokens.shape
    value_size = content_tokens.shape[-1]
    blocks = length // BLOCK

    def split_blocks(array):
        return array.reshape(blocks, BLOCK, heads, array.shape[-1])

    causal = jnp.arange(BLOCK)[:, None] >= jnp.arange(BLOCK)[None, :]
    highest = lax.Precision.HIGHEST

    def step(state, incoming_tokens):
        query_block, key_block, value_block, decay_block = incoming_tokens
        cumulative = jnp.cumsum(decay_block, axis=0)
        differ = cumulative[:, None] - cumulative[None, :]
        weight = jnp.exp(jnp.where(causal[:, :, None, None], differ, -jnp.inf))
        scores = jnp.einsum("thd,shd,tshd->tsh", query_block, key_block, weight, precision=highest)
        inner = jnp.einsum("tsh,shv->thv", scores, value_block, precision=highest)
        carried = jnp.einsum(
            "thd,hdv->thv", query_block * jnp.exp(cumulative), state, precision=highest
        )
        final = cumulative[-1]
        state = jnp.exp(final)[:, :, None] * state + jnp.einsum(
            "shd,shv->hdv",
            key_block * jnp.exp(final[None] - cumulative),
            value_block,
            precision=highest,
        )
        return (state, inner + carried)

    start_state = jnp.zeros((heads, key_size, value_size), jnp.float32)
    _, result_tokens = lax.scan(
        step,
        start_state,
        (
            split_blocks(probe_tokens),
            split_blocks(lookup_tokens),
            split_blocks(content_tokens),
            split_blocks(forgetting_scores),
        ),
    )
    return result_tokens.reshape(length, heads, value_size)


def attend_unit_results(
    probe_tokens,
    lookup_tokens,
    content_tokens,
    result_switch,
    forgetting_raw,
    spike_forgetting,
    attend_unit_scale,
):
    length = probe_tokens.shape[0]
    heads = probe_tokens.shape[1] // HEAD_K
    forgetting_scores = jax.nn.log_sigmoid(forgetting_raw) / switch_multiplier + spike_forgetting

    def split_heads(array, width):
        return array.astype(jnp.float32).reshape(length, heads, width)

    result_tokens = gated_scan(
        split_heads(probe_tokens, HEAD_K) * HEAD_K ** (-0.5),
        split_heads(lookup_tokens, HEAD_K),
        split_heads(content_tokens, HEAD_V),
        split_heads(forgetting_scores, HEAD_K),
    )
    result_tokens = result_tokens * lax.rsqrt(
        jnp.mean(result_tokens * result_tokens, axis=-1, keepdims=True) + norm_eps
    )
    result_tokens = result_tokens * attend_unit_scale.astype(jnp.float32).reshape(heads, HEAD_V)
    switched_result = result_tokens.reshape(length, heads * HEAD_V) * jax.nn.silu(
        result_switch.astype(jnp.float32)
    )
    return switched_result.astype(jnp.bfloat16)


def causal_conv(content_tokens, taps):
    content_tokens = content_tokens.astype(jnp.float32)
    taps = taps.astype(jnp.float32)
    width = taps.shape[0]
    padded = jnp.pad(content_tokens, ((width - 1, 0), (0, 0)))
    total = jnp.zeros_like(content_tokens)
    for offset in range(width):
        total = total + padded[offset : offset + content_tokens.shape[0]] * taps[offset]
    return total


def shards(
    incoming_features,
    attend_prenormal_scale,
    probe_matrix,
    lookup_matrix,
    content_matrix,
    forgetting_matrix,
    result_switch_matrix,
    forgetting_shift,
    spike_forget_logarithm,
    attend_unit_scale,
    attend_result_matrix,
    perceptron_scale,
    content_expand_matrix,
    switch_expand_matrix,
    content_kernel,
    switch_kernel,
    contract_matrix,
):
    local_width = incoming_features.shape[1]
    early_value, early_gate = sent_together(
        (content_expand_matrix, switch_expand_matrix), "fs", 0, 1
    )
    whole_in = gather_directly(incoming_features, "tp", 1)
    normed = row_norm(whole_in, attend_prenormal_scale)
    pieces = sent_together(
        (probe_matrix, lookup_matrix, content_matrix, forgetting_matrix, result_switch_matrix),
        "fs",
        0,
        1,
    )
    query_sum, key_sum, value_sum, decay_sum, gate_sum = tuple(
        (jnp.dot(normed, piece, preferred_element_type=jnp.float32) for piece in pieces)
    )
    switched_result = attend_unit_results(
        query_sum.astype(jnp.bfloat16),
        key_sum.astype(jnp.bfloat16),
        value_sum.astype(jnp.bfloat16),
        gate_sum.astype(jnp.bfloat16),
        decay_sum + forgetting_shift,
        spike_forget_logarithm,
        attend_unit_scale,
    )
    mixer_partial = jnp.dot(
        switched_result,
        gather_directly(attend_result_matrix, "fs", 1),
        preferred_element_type=jnp.float32,
    )
    mix = (
        taken_together(mixer_partial.astype(jnp.bfloat16), "tp")
        .astype(jnp.float32)
        .astype(jnp.bfloat16)
    )
    whole_mid = (
        whole_in.astype(jnp.float32) + lax.optimization_barrier(mix).astype(jnp.float32)
    ).astype(jnp.bfloat16)
    offset = lax.axis_index("tp") * local_width
    middle = lax.dynamic_slice_in_dim(whole_mid, offset, local_width, 1)
    normed_mid = row_norm(whole_mid, perceptron_scale)
    value_total = jnp.dot(normed_mid, early_value, preferred_element_type=jnp.float32)
    gate_total = jnp.dot(normed_mid, early_gate, preferred_element_type=jnp.float32)
    conv_value = causal_conv(value_total.astype(jnp.bfloat16), content_kernel)
    conv_gated = causal_conv(gate_total.astype(jnp.bfloat16), switch_kernel)
    hidden = (conv_value * jax.nn.gelu(conv_gated, approximate=True)).astype(jnp.bfloat16)
    down_partial = jnp.dot(
        hidden, gather_directly(contract_matrix, "fs", 1), preferred_element_type=jnp.float32
    )
    ffn = summed_on_arrival(down_partial.astype(jnp.bfloat16), "tp", 1).astype(jnp.bfloat16)
    return (middle.astype(jnp.float32) + lax.optimization_barrier(ffn).astype(jnp.float32)).astype(
        jnp.bfloat16
    )


def solution(mesh):
    placed = (
        P(("rep", "fs"), "tp"),
        P(),
        P("fs", "tp"),
        P("fs", "tp"),
        P("fs", "tp"),
        P("fs", "tp"),
        P("fs", "tp"),
        P("tp"),
        P(("rep", "fs"), "tp"),
        P("tp"),
        P("tp", "fs"),
        P(),
        P("fs", "tp"),
        P("fs", "tp"),
        P(None, "tp"),
        P(None, "tp"),
        P("tp", "fs"),
    )
    return jax.shard_map(
        shards, mesh=mesh, in_specs=placed, out_specs=P(("rep", "fs"), "tp"), check_vma=False
    )
```

profile of v0, /device:TPU:1, one launch (start us, length us, event | category | flops | bytes accessed | tf_op | source)
XLA Modules:
  0.0 545.7 jit_solution(4321324223914472959)
XLA Ops:
  8.1 1.8 broadcast_in_dim.32
  9.9 10.3 %all-to-all-start = ((bf16[8,192,256]{2,1,0:T(8,128)(2,1)}), bf16[8,192,256]{2,1,0:T(8,128)(2,1)S(1)}, u32[]{:S(2)}, u32[]{:S(2)}) async-start(bf16[8,192,256]{2,1,0:T(8,128)(2,1)} %broadcast_in_dim.32), calls=%async_computation | async-start | bytes 1572864 | tf_op jit(solution)/shard_map/all_to_all | solution.py:26
  20.3 12.2 %all-to-all-done = bf16[8,192,256]{2,1,0:T(8,128)(2,1)S(1)} async-done(((bf16[8,192,256]{2,1,0:T(8,128)(2,1)}), bf16[8,192,256]{2,1,0:T(8,128)(2,1)S(1)}, u32[]{:S(2)}, u32[]{:S(2)}) %all-to-all-start) | async-done | bytes 786464 | tf_op jit(solution)/shard_map/all_to_all | solution.py:26
  33.3 10.9 %all-to-all-start.1 = ((bf16[32,128,64]{1,2,0:T(8,128)(2,1)}), bf16[32,128,64]{1,2,0:T(8,128)(2,1)}, u32[]{:S(2)}, u32[]{:S(2)}) async-start(bf16[32,128,64]{1,2,0:T(8,128)(2,1)} %broadcast_in_dim.35), calls=%async_computation.1 | async-start | bytes 1048576 | tf_op jit(solution)/shard_map/all_to_all | solution.py:26
  46.0 170.9 %all-gather.3.cloned.1.call-done = bf16[2048,448]{1,0:T(8,128)(2,1)} async-done(((bf16[64,448]{1,0:T(8,128)(2,1)}), bf16[2048,448]{1,0:T(8,128)(2,1)}) %all-gather.3.cloned.1.call-update) | async-done | bytes 1835024 | tf_op jit(solution)/shard_map/all_gather | solution.py:17
  222.8 24.4 %while.13 = (s32[]{:T(128)}, f32[2,32,64]{2,1,0:T(8,128)S(1)}, f32[3,64,2,64]{1,3,2,0:T(8,128)}, f32[3,64,2,32]{1,0,3,2:T(4,128)S(1)}, f32[3,64,2,32]{1,0,3,2:T(...) while((s32[]{:T(128)}, f32[2,32,64]{2,1,0:T(8,128)S(1)}, ...), condition=%wide.region_3.4_spmd.clone, body=%wide.region_1.3_spmd.clone.sunk | while | flops 14184451 | bytes 5089396 | solution.py:96
  223.1 1.7 select_exponential_fusion.2
  224.9 2.4 copy.143
  231.3 1.7 select_exponential_fusion.2
  233.0 2.4 copy.143
  239.4 1.7 select_exponential_fusion.2
  241.2 2.4 copy.143
  249.7 2.1 convolution_convert_fusion.1
  251.8 3.4 broadcast_in_dim.36
  255.3 27.8 %all-to-all-start.2 = ((bf16[8,192,2048]{2,1,0:T(8,128)(2,1)}), bf16[8,192,2048]{2,1,0:T(8,128)(2,1)}, u32[]{:S(2)}, u32[]{:S(2)}) async-start(bf16[8,192,2048]{2,1,0:T(8,128)(2,1)} %broadcast_in_dim.36), calls=%async_computation.2 | async-start | bytes 12582912 | tf_op jit(solution)/shard_map/all_to_all | solution.py:26
  283.8 70.5 %all-to-all-done.2 = bf16[8,192,2048]{2,1,0:T(8,128)(2,1)} async-done(((bf16[8,192,2048]{2,1,0:T(8,128)(2,1)}), bf16[8,192,2048]{2,1,0:T(8,128)(2,1)}, u32[]{:S(2)}, u32[]{:S(2)}) %all-to-all-start.2) | async-done | bytes 6291488 | tf_op jit(solution)/shard_map/all_to_all | solution.py:26
  354.3 1.6 broadcast_in_dim.37
  356.0 11.2 %all-to-all-start.3 = ((bf16[32,512,64]{1,2,0:T(8,128)(2,1)}), bf16[32,512,64]{1,2,0:T(8,128)(2,1)}, u32[]{:S(2)}, u32[]{:S(2)}) async-start(bf16[32,512,64]{1,2,0:T(8,128)(2,1)} %broadcast_in_dim.37), calls=%async_computation.3 | async-start | bytes 4194304 | tf_op jit(solution)/shard_map/all_to_all | solution.py:26
  367.2 4.2 reduce_sum.53
  371.7 122.6 %all-gather.5.cloned.1.call-done = bf16[2048,1024]{1,0:T(8,128)(2,1)} async-done(((bf16[64,1024]{1,0:T(8,128)(2,1)}), bf16[2048,1024]{1,0:T(8,128)(2,1)}) %all-gather.5.cloned.1.call-update) | async-done | bytes 4194320 | tf_op jit(solution)/shard_map/all_gather | solution.py:17
  494.3 2.4 fusion.32
  497.8 2.6 convolution_convert_fusion
  501.3 24.5 %all-to-all-start.4 = ((bf16[8,192,256]{2,1,0:T(8,128)(2,1)}), bf16[8,192,256]{2,1,0:T(8,128)(2,1)S(1)}, u32[]{:S(2)}, u32[]{:S(2)}) async-start(bf16[8,192,256]{2,1,0:T(8,128)(2,1)} %bitcast.78), calls=%async_computation.4 | async-start | bytes 1572864 | tf_op jit(solution)/shard_map/all_to_all | solution.py:53
  525.9 12.2 %all-to-all-done.4 = bf16[8,192,256]{2,1,0:T(8,128)(2,1)S(1)} async-done(((bf16[8,192,256]{2,1,0:T(8,128)(2,1)}), bf16[8,192,256]{2,1,0:T(8,128)(2,1)S(1)}, u32[]{:S(2)}, u32[]{:S(2)}) %all-to-all-start.4) | async-done | bytes 786464 | tf_op jit(solution)/shard_map/all_to_all | solution.py:53
  (127 shorter events, 28.3 us)
Async XLA Ops:
  6.5 13.7 %copy-start.10 = (bf16[2048]{0:T(1024)(128)(2,1)S(1)}, bf16[2048]{0:T(1024)(128)(2,1)}, u32[]{:S(2)}) copy-start(bf16[2048]{0:T(1024)(128)(2,1)} %param.20) | copy-start | bytes 12292
  6.5 13.7 %copy-start.14 = (bf16[128]{0:T(256)(128)(2,1)S(1)}, bf16[128]{0:T(256)(128)(2,1)}, u32[]{:S(2)}) copy-start(bf16[128]{0:T(256)(128)(2,1)} %param.28) | copy-start | bytes 772
  6.5 25.9 %copy-start.7 = (bf16[128,64]{0,1:T(8,128)(2,1)S(1)}, bf16[128,64]{0,1:T(8,128)(2,1)}, u32[]{:S(2)}) copy-start(bf16[128,64]{0,1:T(8,128)(2,1)} %param.29) | copy-start | bytes 49156
  6.5 210.4 %all-gather.3.cloned.1.call-start = ((), (), s32[]{:S(2)}) async-start(), calls=%async_computation.5 | async-start | bytes 2162688 | tf_op jit(solution)/shard_map/all_gather | solution.py:17
  9.9 22.5 %all-to-all-start = ((bf16[8,192,256]{2,1,0:T(8,128)(2,1)}), bf16[8,192,256]{2,1,0:T(8,128)(2,1)S(1)}, u32[]{:S(2)}, u32[]{:S(2)}) async-start(bf16[8,192,256]{2,1,0:T(8,128)(2,1)} %broadcast_in_dim.32), calls=%async_computation | async-start | bytes 1572864 | tf_op jit(solution)/shard_map/all_to_all | solution.py:26
  33.3 216.3 %all-to-all-start.1 = ((bf16[32,128,64]{1,2,0:T(8,128)(2,1)}), bf16[32,128,64]{1,2,0:T(8,128)(2,1)}, u32[]{:S(2)}, u32[]{:S(2)}) async-start(bf16[32,128,64]{1,2,0:T(8,128)(2,1)} %broadcast_in_dim.35), calls=%async_computation.1 | async-start | bytes 1048576 | tf_op jit(solution)/shard_map/all_to_all | solution.py:26
  44.5 1.2 copy-start
  45.9 176.4 %copy-start.6 = (f32[192,64]{0,1:T(8,128)S(1)}, f32[192,64]{0,1:T(8,128)}, u32[]{:S(2)}) copy-start(f32[192,64]{0,1:T(8,128)} %param.27) | copy-start | bytes 147460
  45.9 176.3 %copy-start.12 = (f32[64]{0:T(128)S(1)}, f32[64]{0:T(128)}, u32[]{:S(2)}) copy-start(f32[64]{0:T(128)} %param.26) | copy-start | bytes 772
  216.9 3.9 copy-start.2
  255.3 27.8 %copy-start.4 = (bf16[64,512]{1,0:T(8,128)(2,1)S(1)}, bf16[64,512]{1,0:T(8,128)(2,1)}, u32[]{:S(2)}) copy-start(bf16[64,512]{1,0:T(8,128)(2,1)} %param.32) | copy-start | bytes 196612
  255.3 27.8 %copy-start.5 = (bf16[64,512]{1,0:T(8,128)(2,1)S(1)}, bf16[64,512]{1,0:T(8,128)(2,1)}, u32[]{:S(2)}) copy-start(bf16[64,512]{1,0:T(8,128)(2,1)} %param.31) | copy-start | bytes 196612
  255.3 99.1 %copy-start.3 = (bf16[512,64]{0,1:T(8,128)(2,1)S(1)}, bf16[512,64]{0,1:T(8,128)(2,1)}, u32[]{:S(2)}) copy-start(bf16[512,64]{0,1:T(8,128)(2,1)} %param.35) | copy-start | bytes 196612
  255.3 99.1 %all-to-all-start.2 = ((bf16[8,192,2048]{2,1,0:T(8,128)(2,1)}), bf16[8,192,2048]{2,1,0:T(8,128)(2,1)}, u32[]{:S(2)}, u32[]{:S(2)}) async-start(bf16[8,192,2048]{2,1,0:T(8,128)(2,1)} %broadcast_in_dim.36), calls=%async_computation.2 | async-start | bytes 12582912 | tf_op jit(solution)/shard_map/all_to_all | solution.py:26
  283.1 211.3 %all-gather.5.cloned.1.call-start = ((), (), s32[]{:S(2)}) async-start(), calls=%async_computation.6 | async-start | bytes 4325376 | tf_op jit(solution)/shard_map/all_gather | solution.py:17
  356.0 11.2 %copy-start.11 = (bf16[2048]{0:T(1024)(128)(2,1)S(1)}, bf16[2048]{0:T(1024)(128)(2,1)}, u32[]{:S(2)}) copy-start(bf16[2048]{0:T(1024)(128)(2,1)} %param.30) | copy-start | bytes 12292
  356.0 11.2 %copy-start.8 = (bf16[3,512]{1,0:T(4,128)(2,1)S(1)}, bf16[3,512]{1,0:T(4,128)(2,1)}, u32[]{:S(2)}) copy-start(bf16[3,512]{1,0:T(4,128)(2,1)} %param.34) | copy-start | bytes 9220
  356.0 11.2 %copy-start.9 = (bf16[3,512]{1,0:T(4,128)(2,1)S(1)}, bf16[3,512]{1,0:T(4,128)(2,1)}, u32[]{:S(2)}) copy-start(bf16[3,512]{1,0:T(4,128)(2,1)} %param.33) | copy-start | bytes 9220
  356.0 141.8 %all-to-all-start.3 = ((bf16[32,512,64]{1,2,0:T(8,128)(2,1)}), bf16[32,512,64]{1,2,0:T(8,128)(2,1)}, u32[]{:S(2)}, u32[]{:S(2)}) async-start(bf16[32,512,64]{1,2,0:T(8,128)(2,1)} %broadcast_in_dim.37), calls=%async_computation.3 | async-start | bytes 4194304 | tf_op jit(solution)/shard_map/all_to_all | solution.py:26
  367.2 4.2 copy-start.1
  494.3 2.8 copy-start.13
  501.3 36.7 %all-to-all-start.4 = ((bf16[8,192,256]{2,1,0:T(8,128)(2,1)}), bf16[8,192,256]{2,1,0:T(8,128)(2,1)S(1)}, u32[]{:S(2)}, u32[]{:S(2)}) async-start(bf16[8,192,256]{2,1,0:T(8,128)(2,1)} %bitcast.78), calls=%async_computation.4 | async-start | bytes 1572864 | tf_op jit(solution)/shard_map/all_to_all | solution.py:53
Sparse Core Ops, SparseCore 0:
  9.4 207.4 all-gather.2
  285.9 208.3 all-gather.4
where the time goes:
time: 547 us; the launch traced here: 546 us
  waiting for transfers between devices  388 us (71%)
  starting transfers between devices  84.7 us (15%)
  local copies, waits for them, and re-layouts  27 us (5%)
  matrix products  16.3 us (3%)
  other arithmetic  15.3 us (3%)
  between operations  13.7 us (3%)
    all_gather x2, waiting for transfers between devices, sent_together(): result, at, outs = (lax.all_gather(both, axis, axis=dim, tiled=True), 0, [])  294 us
    all_to_all x4, waiting for transfers between devices, sent_to_all(): lax.all_to_all(jnp.broadcast_to(array[None], (devices, *array.shape)), ax...  82.7 us
    all_to_all x4, starting transfers between devices, sent_to_all(): lax.all_to_all(jnp.broadcast_to(array[None], (devices, *array.shape)), ax...  60.1 us
    all_to_all x1, starting transfers between devices, summed_on_arrival(): lax.all_to_all(split_up(array, dim, devices), axis, 0, 0, tiled=True)  24.5 us
    all_to_all x1, waiting for transfers between devices, summed_on_arrival(): lax.all_to_all(split_up(array, dim, devices), axis, 0, 0, tiled=True)  12.2 us
  transfers between devices with their start and end apart: 7, of which 5 were waited for; matrix products, arithmetic and copies ran while one was open for 8% of the time, Pallas kernels for 0%

commit v1 on v0

v1 whole, which is shorter than its diff:
```python
import functools
import heapq

import jax
import jax.numpy as jnp
from jax import lax
from jax.experimental import pallas as pl
from jax.experimental.pallas import tpu as pltpu
from jax.sharding import PartitionSpec as P

HEAD_K = 32
HEAD_V = 64
SUB = 16
NEVER = -1e30
norm_eps = 1e-06
MESH = pl.DeviceIdType.MESH
WIDTH = 2176
PARTS = (
    (0, "A", 0, 256),
    (0, "B", 256, 640),
    (1, "A", 640, 1280),
    (1, "B", 1280, 2176),
)
LENGTH = 192
GROUP = 8
COLS = 256
GELU = 0.7978845608028654

ROWS = 64
SIZES = {"y": 4, "z": 8}


def tree_messages(cls, tree, lo, hi):
    first, second = ("y", "z") if tree == "A" else ("z", "y")
    msgs = []

    def chain(axis, base, r0, rn, dep, stage):
        n = SIZES[axis]
        made = []
        for sign in (1, -1):
            d, s = dep, stage
            for k in range(1, n // 2 + 1):
                o = dict(base)
                o[axis] = sign * (k - 1)
                a0, an = r0, rn
                if k == n // 2:
                    an = rn // 2
                    a0 = r0 + (0 if sign > 0 else an)
                m = dict(cls=cls, lo=lo, hi=hi, axis=axis, sign=sign, o=o, r0=a0, rn=an, dep=d, stage=s, off=sign * k)
                msgs.append(m)
                made.append(m)
                d, s = m, s + 1
        return made

    made = chain(first, {"y": 0, "z": 0}, 0, ROWS, None, 0)
    chain(second, {"y": 0, "z": 0}, 0, ROWS, None, 0)
    for m in made:
        chain(second, {first: m["off"], second: 0}, m["r0"], m["rn"], m, m["stage"] + 1)
    return msgs


def plan(parts, rate=46.6e3, lat=1.9, ready=None):
    msgs = []
    for p in parts:
        msgs += tree_messages(*p)
    for i, m in enumerate(msgs):
        m["id"] = i
        m["bytes"] = m["rn"] * (m["hi"] - m["lo"]) * 2
    kids = {}
    for m in msgs:
        kids.setdefault(m["dep"]["id"] if m["dep"] else None, []).append(m)
    depth = {}
    def dep_depth(m):
        if m["id"] not in depth:
            depth[m["id"]] = 1 + max([dep_depth(k) for k in kids.get(m["id"], [])], default=0)
        return depth[m["id"]]
    free = {(a, s): 0.0 for a in "yz" for s in (1, -1)}
    avail = {k: [] for k in free}
    events = [(0.0, 0, m["id"]) for m in kids[None]]
    heapq.heapify(events)
    order = []
    t = 0.0
    pending = sorted(events)
    ev = list(pending)
    heapq.heapify(ev)
    n = 0
    while ev:
        t = ev[0][0]
        while ev and ev[0][0] <= t + 1e-9:
            _, kind, i = heapq.heappop(ev)
            if kind == 0:
                m = msgs[i]
                heapq.heappush(avail[(m["axis"], m["sign"])], (m["cls"], -dep_depth(m), i))
        for link, q in avail.items():
            if q and free[link] <= t + 1e-9:
                _, _, i = heapq.heappop(q)
                m = msgs[i]
                m["start"] = t
                free[link] = t + m["bytes"] / rate
                m["arrive"] = free[link] + lat
                order.append(m)
                heapq.heappush(ev, (free[link], 1, 0))
                for k in kids.get(i, []):
                    heapq.heappush(ev, (m["arrive"], 0, k["id"]))
    return order


def neighbour(axis, sign):
    rep, fs = lax.axis_index("rep"), lax.axis_index("fs")
    y, z = lax.rem(fs, 4), rep * 8 + fs // 4
    if axis == "y":
        y = lax.rem(y + 4 + sign, 4)
    else:
        z = lax.rem(z + 16 + sign, 16)
    return {"rep": z // 8, "fs": lax.rem(z, 8) * 4 + y}


def block_of(o):
    fs = lax.axis_index("fs")
    y, z = lax.rem(fs, 4), fs // 4
    y = lax.rem(y + 8 - o["y"], 4)
    z = lax.rem(z + 16 - o["z"], 8)
    return z * 4 + y


def attention_pieces(q, k, v, g, ld, unit, roll):
    length = q.shape[0]
    blocks = length // SUB
    exact = lax.Precision.HIGHEST
    row = lax.broadcasted_iota(jnp.int32, (length, 64), 0) % SUB
    c = ld
    shift = 1
    while shift < SUB:
        c = c + jnp.where(row >= shift, roll(c, shift), 0.0)
        shift *= 2
    key_head = lax.broadcasted_iota(jnp.int32, (64, 128), 0) // HEAD_K
    value_head = lax.broadcasted_iota(jnp.int32, (64, 128), 1) // HEAD_V
    spread = jnp.where(key_head == value_head, 1.0, 0.0)
    c3 = c.reshape(blocks, SUB, 64)
    total = c3[:, SUB - 1 : SUB, :]
    k_end = (k.reshape(blocks, SUB, 64) * jnp.exp(total - c3))
    q_in = q * jnp.exp(c)
    v3 = v.reshape(blocks, SUB, 128)
    fade = jnp.exp(total)
    q3 = q_in.reshape(blocks, SUB, 64)
    own_head = (
        lax.broadcasted_iota(jnp.int32, (128, 64), 0) // HEAD_V
        == lax.broadcasted_iota(jnp.int32, (128, 64), 1) // HEAD_K
    )
    yield None
    out = jnp.zeros((length, 128), jnp.float32)
    for j in range(SUB):
        if j == 0:
            pairs, values = q * k, v
        else:
            differ = jnp.where(row >= j, c - roll(c, j), NEVER)
            pairs, values = q * roll(k, j) * jnp.exp(differ), roll(v, j)
        scores = jnp.dot(pairs, spread, precision=exact, preferred_element_type=jnp.float32)
        out = out + scores * values
        if j % 4 == 3:
            yield None
    state = None
    carried = [jnp.zeros((SUB, 128), jnp.float32)]
    for i in range(blocks):
        if state is not None:
            carried.append(
                lax.dot_general(
                    q3[i], state, (((1,), (1,)), ((), ())), precision=exact,
                    preferred_element_type=jnp.float32,
                )
            )
        if i < blocks - 1:
            update = lax.dot_general(
                v3[i], k_end[i], (((0,), (0,)), ((), ())), precision=exact,
                preferred_element_type=jnp.float32,
            )
            update = jnp.where(own_head, update, 0.0)
            state = update if state is None else state * fade[i] + update
        if i % 4 == 3:
            yield None
    out = out + jnp.concatenate(carried, axis=0)
    same = jnp.where(
        lax.broadcasted_iota(jnp.int32, (128, 128), 0) // HEAD_V
        == lax.broadcasted_iota(jnp.int32, (128, 128), 1) // HEAD_V,
        1.0 / HEAD_V,
        0.0,
    )
    mean = jnp.dot(out * out, same, precision=exact, preferred_element_type=jnp.float32)
    out = out * lax.rsqrt(mean + norm_eps) * unit * (g / (1.0 + jnp.exp(-g)))
    yield out.astype(jnp.bfloat16)


def rows_norm(blocks, gain_ref, out):
    total = jnp.zeros((LENGTH, COLS), jnp.float32)
    for t in range(GROUP):
        one = blocks[t].astype(jnp.float32)
        total = total + one * one
    mean = jnp.sum(total, axis=1, keepdims=True) * (1.0 / (GROUP * COLS))
    scale = lax.rsqrt(mean + norm_eps)
    for t in range(GROUP):
        at = slice(t * COLS, (t + 1) * COLS)
        gain = gain_ref[:, at].astype(jnp.float32)
        out[:, at] = (blocks[t].astype(jnp.float32) * scale * gain).astype(jnp.bfloat16)


def short_conv(tokens, taps):
    row = lax.broadcasted_iota(jnp.int32, tokens.shape, 0)
    one = jnp.where(row >= 1, pltpu.roll(tokens, 1, 0), 0.0)
    two = jnp.where(row >= 2, pltpu.roll(tokens, 2, 0), 0.0)
    return two * taps[0:1] + one * taps[1:2] + tokens * taps[2:3]


def layer_kernel(
    order,
    packed_ref,
    x_ref,
    pre_ref,
    shift_ref,
    spike_ref,
    unit_ref,
    post_ref,
    value_taps,
    gate_taps,
    out_ref,
    whole,
    x_all,
    mid_all,
    sums,
    from_partner,
    pair_sums,
    from_chips,
    down_from_partner,
    down_pair_sums,
    down_from_chips,
    normed,
    hidden,
    own_sem,
    send_sem,
    recv_sem,
    tp_send,
    tp_recv,
):
    f32, bf16 = jnp.float32, jnp.bfloat16
    tp = lax.axis_index("tp")
    chip, core = tp // 2, lax.rem(tp, 2)
    partner = chip * 2 + (1 - core)

    def peer(d):
        return lax.rem(chip + 4 + d, 4) * 2 + core

    barrier = pltpu.get_barrier_semaphore()
    for axis in ("y", "z"):
        for sign in (1, -1):
            pl.semaphore_signal(
                barrier, inc=1, device_id=neighbour(axis, sign), device_id_type=MESH
            )
    for other in (peer(1), peer(2), peer(3), partner):
        pl.semaphore_signal(barrier, inc=1, device_id={"tp": other}, device_id_type=MESH)
    mine = pl.multiple_of(lax.axis_index("fs") * ROWS, ROWS)
    own = [
        pltpu.make_async_copy(packed_ref, whole.at[pl.ds(mine, ROWS)], own_sem.at[0]),
        pltpu.make_async_copy(x_ref, x_all.at[tp], own_sem.at[1]),
    ]
    for one in own:
        one.start()
    for one in own:
        one.wait()
    pl.semaphore_wait(barrier, 8)

    def copy_of(m, step):
        o = dict(m["o"])
        o[m["axis"]] = o[m["axis"]] + step * m["sign"]
        row = pl.multiple_of(block_of(o) * ROWS + m["r0"], 16)
        at = whole.at[pl.ds(row, m["rn"]), pl.ds(m["lo"], m["hi"] - m["lo"])]
        return pltpu.make_async_remote_copy(
            src_ref=at,
            dst_ref=at,
            send_sem=send_sem.at[m["id"]],
            recv_sem=recv_sem.at[m["id"]],
            device_id=neighbour(m["axis"], m["sign"]),
            device_id_type=MESH,
        )

    seen, at_message = set(), [0]

    def arrived(m):
        if m["id"] not in seen:
            copy_of(m, 1).wait_recv()
            seen.add(m["id"])

    def pump(until):
        while at_message[0] < len(order) and order[at_message[0]]["start"] <= until:
            m = order[at_message[0]]
            if m["dep"] is not None:
                arrived(m["dep"])
            copy_of(m, 0).start()
            at_message[0] += 1

    def class_arrived(cls):
        mine_of = sorted((m for m in order if m["cls"] == cls), key=lambda m: m["arrive"])
        for m in mine_of:
            pump(m["arrive"])
            arrived(m)
        return mine_of[-1]["arrive"]

    def tp_copy(src, dst, number, to):
        return pltpu.make_async_remote_copy(
            src_ref=src,
            dst_ref=dst,
            send_sem=tp_send.at[number],
            recv_sem=tp_recv.at[number],
            device_id={"tp": to},
            device_id_type=MESH,
        )

    started = []

    def begin(copy):
        copy.start()
        started.append(copy)

    def share(buf, base):
        for d in (2, 1, 3):
            begin(tp_copy(buf.at[tp], buf.at[tp], base + d - 1, peer(d)))
        begin(tp_copy(buf.at[tp], buf.at[tp], base + 3, partner))

    def share_on(buf, base):
        for d in (1, 3, 2):
            came = buf.at[peer(-d)]
            tp_copy(came, came, base + d - 1, peer(d)).wait_recv()
            begin(tp_copy(came, came, base + 3 + d, partner))

    def shared(buf, base):
        for d in range(4):
            came = buf.at[lax.rem(chip + 4 - d, 4) * 2 + (1 - core)]
            tp_copy(came, came, base + 3 + d, partner).wait_recv()

    def summed(product, got, paired, chips, base, clock):
        waiting = []
        for d in (2, 1, 3, 0):
            there = lax.rem(chip + d, 4) * 2
            for who in (1 - core, core):
                sums[there + who] = product(there + who).astype(bf16)
            for copy in waiting:
                begin(copy)
            waiting = [tp_copy(sums.at[there + 1 - core], got.at[d], base + d, partner)]
            pump(clock(d))
        for copy in waiting:
            begin(copy)
        waiting = []
        for d in (2, 1, 3):
            there = lax.rem(chip + d, 4) * 2 + core
            tp_copy(sums.at[there], got.at[d], base + d, partner).wait_recv()
            paired[d - 1] = (sums[there].astype(f32) + got[d].astype(f32)).astype(bf16)
            for copy in waiting:
                begin(copy)
            waiting = [tp_copy(paired.at[d - 1], chips.at[d - 1], base + 3 + d, peer(d))]
        tp_copy(sums.at[tp], got.at[0], base, partner).wait_recv()
        for copy in waiting:
            begin(copy)
        total = sums[tp].astype(f32) + got[0].astype(f32)
        return total

    def chips_added(total, chips, base):
        for d in (1, 3, 2):
            tp_copy(chips.at[d - 1], chips.at[d - 1], base + 3 + d, peer(d)).wait_recv()
            total = total + chips[d - 1].astype(f32)
        return total

    last = order[-1]["start"]
    share(x_all, 0)
    pump(T_SHARE)
    share_on(x_all, 0)
    pump(T_SHARED)
    shared(x_all, 0)
    rows_norm(x_all, pre_ref, normed)
    now = class_arrived(0)

    first = jnp.dot(normed[...], whole[:, 0:256], preferred_element_type=f32)
    second = jnp.dot(normed[...], whole[:, 256:512], preferred_element_type=f32)
    pump(now + 2.0)
    rounded = first.astype(bf16).astype(f32)
    query = rounded[:, 0:64] * HEAD_K ** (-0.5)
    key = rounded[:, 64:128]
    value = rounded[:, 128:256]
    gate = second[:, 0:128].astype(bf16).astype(f32)
    forget = second[:, 128:192] + shift_ref[...]
    decay = -(jnp.maximum(-forget, 0.0) + jnp.log1p(jnp.exp(-jnp.abs(forget)))) / 16.0
    decay = decay + spike_ref[...]
    unit = unit_ref[...].astype(f32)
    now = now + 2.0
    for piece in attention_pieces(
        query, key, value, gate, decay, unit, lambda a, s: pltpu.roll(a, s, 0)
    ):
        now = now + T_PIECE
        pump(now)
        gated = piece

    def mix_part(t):
        rows = pl.ds(pl.multiple_of(t * COLS, COLS), COLS)
        return lax.dot_general(
            gated, whole[rows, 512:640], (((1,), (1,)), ((), ())), preferred_element_type=f32
        )

    begun = now
    total = summed(mix_part, from_partner, pair_sums, from_chips, 8, lambda d: begun + 2.0)
    pump(begun + 5.0)
    mix = chips_added(total, from_chips, 8).astype(bf16)
    mid_all[tp] = (x_all[tp].astype(f32) + mix.astype(f32)).astype(bf16)
    pump(begun + 9.0)
    share(mid_all, 16)
    pump(begun + 12.0)
    share_on(mid_all, 16)
    pump(begun + 15.0)
    shared(mid_all, 16)
    rows_norm(mid_all, post_ref, normed)
    pump(last)
    class_arrived(1)

    for block in range(4):
        at = block * 128
        cols = slice(at, at + 128)
        up_value = jnp.dot(
            normed[...], whole[:, 640 + at : 768 + at], preferred_element_type=f32
        )
        up_gate = jnp.dot(
            normed[...], whole[:, 1152 + at : 1280 + at], preferred_element_type=f32
        )
        conv_value = short_conv(up_value.astype(bf16).astype(f32), value_taps[:, cols].astype(f32))
        conv_gate = short_conv(up_gate.astype(bf16).astype(f32), gate_taps[:, cols].astype(f32))
        cube = conv_gate + 0.044715 * (conv_gate * conv_gate * conv_gate)
        gelu = conv_gate * (0.5 * (1.0 + jnp.tanh(GELU * cube)))
        hidden[:, cols] = (conv_value * gelu).astype(bf16)

    def down_part(t):
        rows = pl.ds(pl.multiple_of(t * COLS, COLS), COLS)
        return lax.dot_general(
            hidden[...], whole[rows, 1664:2176], (((1,), (1,)), ((), ())), preferred_element_type=f32
        )

    for copy in started[7:14]:
        copy.wait_send()
    total = summed(down_part, down_from_partner, down_pair_sums, down_from_chips, 24, lambda d: last)
    ffn = chips_added(total, down_from_chips, 24).astype(bf16)
    out_ref[...] = (mid_all[tp].astype(f32) + ffn.astype(f32)).astype(bf16)

    for copy in started[:7] + started[14:]:
        copy.wait_send()
    for m in order:
        copy_of(m, 0).wait_send()


T_SHARE = 4.0
T_SHARED = 9.0
T_PIECE = 0.7


def shards(
    incoming_features,
    attend_prenormal_scale,
    probe_matrix,
    lookup_matrix,
    content_matrix,
    forgetting_matrix,
    result_switch_matrix,
    forgetting_shift,
    spike_forget_logarithm,
    attend_unit_scale,
    attend_result_matrix,
    perceptron_scale,
    content_expand_matrix,
    switch_expand_matrix,
    content_kernel,
    switch_kernel,
    contract_matrix,
):
    packed = jnp.concatenate(
        (
            probe_matrix,
            lookup_matrix,
            content_matrix,
            result_switch_matrix,
            forgetting_matrix,
            jnp.zeros_like(forgetting_matrix),
            attend_result_matrix.T,
            content_expand_matrix,
            switch_expand_matrix,
            contract_matrix.T,
        ),
        axis=1,
    )
    order = plan(PARTS, rate=42e3, lat=2.5)
    count = len(order)
    block = (LENGTH, COLS)
    dma = pltpu.SemaphoreType.DMA
    vmem = pl.BlockSpec(memory_space=pltpu.VMEM)
    hbm = pl.BlockSpec(memory_space=pl.ANY)
    bf16 = jnp.bfloat16
    return pl.pallas_call(
        functools.partial(layer_kernel, order),
        out_shape=jax.ShapeDtypeStruct(block, bf16),
        in_specs=[hbm, hbm] + [vmem] * 7,
        out_specs=vmem,
        scratch_shapes=[
            pltpu.VMEM((32 * ROWS, WIDTH), bf16),
            pltpu.VMEM((GROUP, *block), bf16),
            pltpu.VMEM((GROUP, *block), bf16),
            pltpu.VMEM((GROUP, *block), bf16),
            pltpu.VMEM((4, *block), bf16),
            pltpu.VMEM((3, *block), bf16),
            pltpu.VMEM((3, *block), bf16),
            pltpu.VMEM((4, *block), bf16),
            pltpu.VMEM((3, *block), bf16),
            pltpu.VMEM((3, *block), bf16),
            pltpu.VMEM((LENGTH, GROUP * COLS), bf16),
            pltpu.VMEM((LENGTH, 512), bf16),
            dma((2,)),
            dma((count,)),
            dma((count,)),
            dma((32,)),
            dma((32,)),
        ],
        compiler_params=pltpu.CompilerParams(
            collective_id=0, has_side_effects=True, vmem_limit_bytes=48 * 1024 * 1024
        ),
    )(
        packed,
        incoming_features,
        attend_prenormal_scale[None],
        forgetting_shift[None],
        spike_forget_logarithm,
        attend_unit_scale[None],
        perceptron_scale[None],
        content_kernel,
        switch_kernel,
    )


def solution(mesh):
    placed = (
        P(("rep", "fs"), "tp"),
        P(),
        P("fs", "tp"),
        P("fs", "tp"),
        P("fs", "tp"),
        P("fs", "tp"),
        P("fs", "tp"),
        P("tp"),
        P(("rep", "fs"), "tp"),
        P("tp"),
        P("tp", "fs"),
        P(),
        P("fs", "tp"),
        P("fs", "tp"),
        P(None, "tp"),
        P(None, "tp"),
        P("tp", "fs"),
    )
    return jax.shard_map(
        shards, mesh=mesh, in_specs=placed, out_specs=P(("rep", "fs"), "tp"), check_vma=False
    )
```

time: 547 us -> 89.2 us (0.16)
  waiting for transfers between devices: 388 us -> 0 us
  Pallas kernels: 0 us -> 84.8 us
  starting transfers between devices: 84.7 us -> 0 us
  local copies, waits for them, and re-layouts: 27 us -> 4.01 us
  matrix products: 16.3 us -> 0 us
  other arithmetic: 15.3 us -> 0 us
  between operations: 13.7 us -> 0.14 us
    all_gather x2 -> x0, waiting for transfers between devices: 294 us -> none  [sent_together(): result, at, outs = (lax.all_gather(both, axis, axis=dim, tiled=True), 0, [])]
    all_to_all x5 -> x0, waiting for transfers between devices: 94.9 us -> none  [the longest x4 82.7 us: sent_to_all(): lax.all_to_all(jnp.broadcast_to(array[None], (devices, *array.shape)), ax...]
    pallas_call x0 -> x1, Pallas kernels: none -> 84.8 us  [shards(): pl.pallas_call(functools.partial(layer_kernel, order), out_shape=jax.Shap...]
    all_to_all x5 -> x0, starting transfers between devices: 84.7 us -> none  [the longest x4 60.1 us: sent_to_all(): lax.all_to_all(jnp.broadcast_to(array[None], (devices, *array.shape)), ax...]
    dot_general x17 -> x0, matrix products: 16.3 us -> none  [the longest x4 4.09 us: shards(): jnp.dot(normed, piece, preferred_element_type=jnp.float32)]
    while x4 -> x0, local copies, waits for them, and re-layouts: 8.13 us -> none
    broadcast_in_dim x4 -> x3, local copies, waits for them, and re-layouts: 7.79 us -> 1.42 us  [the longest x1 0.73 us: shards(): attend_prenormal_scale[None]]
    reduce_sum x5 -> x0, other arithmetic: 5.81 us -> none  [the longest x1 4.18 us: taken_together(): return sent_to_all(array, axis).astype(jnp.float32).sum(axis=0)]
  transfers between devices with their start and end apart: 7 -> 0, of which waited for: 5 -> 0; matrix products, arithmetic and copies ran while one was open for 8% -> 0% of each run, Pallas kernels for 0% -> 0%
where the time goes in v1:
time: 89.2 us; the launch traced here: 88.9 us
  Pallas kernels  84.8 us (95%)
  local copies, waits for them, and re-layouts  4.01 us (4%)
    pallas_call x1, Pallas kernels, shards(): pl.pallas_call(functools.partial(layer_kernel, order), out_shape=jax.Shap...  84.8 us

profile of v1, /device:TPU:1, one launch (start us, length us, event | category | flops | bytes accessed | tf_op | source)
XLA Modules:
  0.0 88.9 jit_solution(1138263072052453120)
XLA Ops:
  0.0 0.0 copy-start.8
  0.0 0.0 copy-start.7
  0.0 0.7 broadcast_in_dim.16.pre_ref
  0.7 0.7 broadcast_in_dim.19.post_ref
  1.4 0.0 copy-start.5
  1.4 0.0 copy-start.6
  1.4 1.0 %copy.18.spike_ref = f32[192,64]{1,0:T(8,128)S(1)} copy(f32[192,64]{0,1:T(8,128)} %param.25) | data formatting | bytes 98304 | tf_op args[8]
  2.4 0.0 copy-done.8
  2.4 0.0 copy-done.7
  2.4 0.0 copy-done.5
  2.4 0.0 copy-done.6
  2.5 0.0 copy-start
  2.5 0.0 copy-start.1
  2.5 0.0 copy-start.2
  2.5 0.0 copy-start.3
  2.5 0.0 copy-start.4
  2.5 0.9 %concatenate.3.packed_ref = bf16[64,2176]{1,0:T(8,128)(2,1)S(1)} concatenate(bf16[64,64]{1,0:T(8,128)(2,1)S(1)} %copy-done.8, bf16[64,64]{1,0:T(8,128)(2,1)} %param.20, bf16[64,128]{1,0:T(8,128)(2,1)} %param.21, bf16[64,128]{1,0:T(8,128)(2,1)} %param.23, bf16[64,64]{1,0:T(8,128)(2,1)} %param.22, bf16[64,64]{1,0:T(8,128)(2,1)S(1)} %broadcast_in_dim.15, bf16[64,128]{1,0:T(8,128)(2,1)} %bitcast.7, ...), dimensions={1} | concatenate | bytes 557056 | tf_op jit(solution)/shard_map/concatenate | solution.py:477
  3.4 0.0 copy-done
  3.5 0.0 copy-done.1
  3.5 0.0 copy-done.2
  3.5 0.0 copy-done.3
  3.5 0.0 copy-done.4
  3.5 84.8 %shard_map.163 = bf16[192,256]{1,0:T(8,128)(2,1)S(1)} custom-call(bf16[64,2176]{1,0:T(8,128)(2,1)S(1)} %concatenate.3.packed_ref, bf16[192,256]{1,0:T(8,128)(2,1)S(1)} %copy-done, bf16[1,2048]{1,0:T(2,128)(2,1)S(1)} %broadcast_in_dim.16.pre_ref, f32[1,64]{1,0:T(1,128)S(1)} %bitcast.4, f32[192,64]{1,0:T(8,128)S(1)} %copy.18.spike_ref, ...), custom_call_target="tpu_custom_call" | custom-call | tf_op jit(solution)/shard_map/pallas_call | solution.py:499
  88.3 0.6 copy.20
  (1 shorter events, 0.0 us)
Async XLA Ops:
  0.0 2.4 %copy-start.8 = (bf16[64,64]{1,0:T(8,128)(2,1)S(1)}, bf16[64,64]{1,0:T(8,128)(2,1)}, u32[]{:S(2)}) copy-start(bf16[64,64]{1,0:T(8,128)(2,1)} %param.19) | copy-start | bytes 24580
  0.0 2.4 %copy-start.7 = (bf16[512,64]{0,1:T(8,128)(2,1)S(1)}, bf16[512,64]{0,1:T(8,128)(2,1)}, u32[]{:S(2)}) copy-start(bf16[512,64]{0,1:T(8,128)(2,1)} %param.33) | copy-start | bytes 196612
  1.4 1.0 %copy-start.5 = (bf16[64,512]{1,0:T(8,128)(2,1)S(1)}, bf16[64,512]{1,0:T(8,128)(2,1)}, u32[]{:S(2)}) copy-start(bf16[64,512]{1,0:T(8,128)(2,1)} %param.29) | copy-start | bytes 196612
  1.4 1.0 %copy-start.6 = (bf16[64,512]{1,0:T(8,128)(2,1)S(1)}, bf16[64,512]{1,0:T(8,128)(2,1)}, u32[]{:S(2)}) copy-start(bf16[64,512]{1,0:T(8,128)(2,1)} %param.30) | copy-start | bytes 196612
  2.5 1.0 %copy-start = (bf16[192,256]{1,0:T(8,128)(2,1)S(1)}, bf16[192,256]{1,0:T(8,128)(2,1)}, u32[]{:S(2)}) copy-start(bf16[192,256]{1,0:T(8,128)(2,1)} %x_ref.1) | copy-start | bytes 294916
  2.5 1.0 %copy-start.1 = (bf16[3,512]{1,0:T(4,128)(2,1)S(1)}, bf16[3,512]{1,0:T(4,128)(2,1)}, u32[]{:S(2)}) copy-start(bf16[3,512]{1,0:T(4,128)(2,1)} %value_taps.1) | copy-start | bytes 9220
  2.5 1.0 %copy-start.2 = (bf16[3,512]{1,0:T(4,128)(2,1)S(1)}, bf16[3,512]{1,0:T(4,128)(2,1)}, u32[]{:S(2)}) copy-start(bf16[3,512]{1,0:T(4,128)(2,1)} %gate_taps.1) | copy-start | bytes 9220
  2.5 1.0 %copy-start.3 = (f32[64]{0:T(128)S(1)}, f32[64]{0:T(128)}, u32[]{:S(2)}) copy-start(f32[64]{0:T(128)} %param.24) | copy-start | bytes 772
  2.5 1.0 %copy-start.4 = (bf16[128]{0:T(256)(128)(2,1)S(1)}, bf16[128]{0:T(256)(128)(2,1)}, u32[]{:S(2)}) copy-start(bf16[128]{0:T(256)(128)(2,1)} %param.26) | copy-start | bytes 772

commit v2 on v1

--- a/solution.py
+++ b/solution.py
@@ -34,74 +34,79 @@
     first, second = ("y", "z") if tree == "A" else ("z", "y")
     msgs = []
 
-    def chain(axis, base, r0, rn, dep, stage):
+    def chain(axis, base, deps, stage):
         n = SIZES[axis]
         made = []
         for sign in (1, -1):
-            d, s = dep, stage
+            d, s = deps, stage
             for k in range(1, n // 2 + 1):
                 o = dict(base)
                 o[axis] = sign * (k - 1)
-                a0, an = r0, rn
+                r0, rn = 0, ROWS
                 if k == n // 2:
-                    an = rn // 2
-                    a0 = r0 + (0 if sign > 0 else an)
-                m = dict(cls=cls, lo=lo, hi=hi, axis=axis, sign=sign, o=o, r0=a0, rn=an, dep=d, stage=s, off=sign * k)
+                    rn = ROWS // 2
+                    r0 = 0 if sign > 0 else rn
+                m = dict(
+                    cls=cls, lo=lo, hi=hi, axis=axis, sign=sign, o=o, r0=r0, rn=rn, deps=d, off=sign * k, stage=s
+                )
                 msgs.append(m)
                 made.append(m)
-                d, s = m, s + 1
+                d, s = (m,), s + 1
         return made
 
-    made = chain(first, {"y": 0, "z": 0}, 0, ROWS, None, 0)
-    chain(second, {"y": 0, "z": 0}, 0, ROWS, None, 0)
+    made = chain(first, {"y": 0, "z": 0}, (), 0)
+    chain(second, {"y": 0, "z": 0}, (), 0)
+    far = SIZES[first] // 2
     for m in made:
-        chain(second, {first: m["off"], second: 0}, m["r0"], m["rn"], m, m["stage"] + 1)
+        if abs(m["off"]) < far:
+            chain(second, {first: m["off"], second: 0}, (m,), m["stage"] + 1)
+    halves = tuple(m for m in made if abs(m["off"]) == far)
+    chain(second, {first: far, second: 0}, halves, halves[0]["stage"] + 1)
     return msgs
 
 
-def plan(parts, rate=46.6e3, lat=1.9, ready=None):
+def plan(parts, rate, lat, each):
     msgs = []
     for p in parts:
         msgs += tree_messages(*p)
+    kids = {}
     for i, m in enumerate(msgs):
         m["id"] = i
         m["bytes"] = m["rn"] * (m["hi"] - m["lo"]) * 2
-    kids = {}
-    for m in msgs:
-        kids.setdefault(m["dep"]["id"] if m["dep"] else None, []).append(m)
+        m["need"] = len(m["deps"])
+        for d in m["deps"]:
+            kids.setdefault(d["id"], []).append(m)
     depth = {}
-    def dep_depth(m):
+
+    def depth_of(m):
         if m["id"] not in depth:
-            depth[m["id"]] = 1 + max([dep_depth(k) for k in kids.get(m["id"], [])], default=0)
+            depth[m["id"]] = 1 + max((depth_of(k) for k in kids.get(m["id"], ())), default=0)
         return depth[m["id"]]
+
     free = {(a, s): 0.0 for a in "yz" for s in (1, -1)}
     avail = {k: [] for k in free}
-    events = [(0.0, 0, m["id"]) for m in kids[None]]
+    events = [(0.0, 0, m["id"]) for m in msgs if not m["deps"]]
     heapq.heapify(events)
     order = []
-    t = 0.0
-    pending = sorted(events)
-    ev = list(pending)
-    heapq.heapify(ev)
-    n = 0
-    while ev:
-        t = ev[0][0]
-        while ev and ev[0][0] <= t + 1e-9:
-            _, kind, i = heapq.heappop(ev)
+    while events:
+        t = events[0][0]
+        while events and events[0][0] <= t + 1e-9:
+            _, kind, i = heapq.heappop(events)
             if kind == 0:
                 m = msgs[i]
-                heapq.heappush(avail[(m["axis"], m["sign"])], (m["cls"], -dep_depth(m), i))
-        for link, q in avail.items():
-            if q and free[link] <= t + 1e-9:
-                _, _, i = heapq.heappop(q)
-                m = msgs[i]
+                heapq.heappush(avail[(m["axis"], m["sign"])], (m["cls"], -depth_of(m), i))
+        for link, queue in avail.items():
+            if queue and free[link] <= t + 1e-9:
+                m = msgs[heapq.heappop(queue)[2]]
                 m["start"] = t
-                free[link] = t + m["bytes"] / rate
+                free[link] = t + m["bytes"] / rate + each
                 m["arrive"] = free[link] + lat
                 order.append(m)
-                heapq.heappush(ev, (free[link], 1, 0))
-                for k in kids.get(i, []):
-                    heapq.heappush(ev, (m["arrive"], 0, k["id"]))
+                heapq.heappush(events, (free[link], 1, 0))
+                for k in kids.get(m["id"], ()):
+                    k["need"] -= 1
+                    if k["need"] == 0:
+                        heapq.heappush(events, (m["arrive"], 0, k["id"]))
     return order
 
 
@@ -190,7 +195,7 @@
     yield out.astype(jnp.bfloat16)
 
 
-def rows_norm(blocks, gain_ref, out):
+def rows_norm(blocks, gain_ref, which, out):
     total = jnp.zeros((LENGTH, COLS), jnp.float32)
     for t in range(GROUP):
         one = blocks[t].astype(jnp.float32)
@@ -199,7 +204,7 @@
     scale = lax.rsqrt(mean + norm_eps)
     for t in range(GROUP):
         at = slice(t * COLS, (t + 1) * COLS)
-        gain = gain_ref[:, at].astype(jnp.float32)
+        gain = gain_ref[which : which + 1, at].astype(jnp.float32)
         out[:, at] = (blocks[t].astype(jnp.float32) * scale * gain).astype(jnp.bfloat16)
 
 
@@ -213,12 +218,14 @@
 def layer_kernel(
     order,
     packed_ref,
+    value_ref,
+    gate_ref,
+    down_ref,
     x_ref,
-    pre_ref,
+    gains_ref,
     shift_ref,
     spike_ref,
     unit_ref,
-    post_ref,
     value_taps,
     gate_taps,
     out_ref,
@@ -228,9 +235,13 @@
     sums,
     from_partner,
     pair_sums,
+    passing,
+    passed,
     from_chips,
     down_from_partner,
     down_pair_sums,
+    down_passing,
+    down_passed,
     down_from_chips,
     normed,
     hidden,
@@ -254,18 +265,21 @@
             pl.semaphore_signal(
                 barrier, inc=1, device_id=neighbour(axis, sign), device_id_type=MESH
             )
-    for other in (peer(1), peer(2), peer(3), partner):
+    for other in (peer(1), peer(3), partner):
         pl.semaphore_signal(barrier, inc=1, device_id={"tp": other}, device_id_type=MESH)
-    mine = pl.multiple_of(lax.axis_index("fs") * ROWS, ROWS)
+    mine = pl.ds(pl.multiple_of(lax.axis_index("fs") * ROWS, ROWS), ROWS)
     own = [
-        pltpu.make_async_copy(packed_ref, whole.at[pl.ds(mine, ROWS)], own_sem.at[0]),
-        pltpu.make_async_copy(x_ref, x_all.at[tp], own_sem.at[1]),
+        pltpu.make_async_copy(packed_ref, whole.at[mine, pl.ds(0, 640)], own_sem.at[0]),
+        pltpu.make_async_copy(value_ref, whole.at[mine, pl.ds(640, 512)], own_sem.at[1]),
+        pltpu.make_async_copy(gate_ref, whole.at[mine, pl.ds(1152, 512)], own_sem.at[2]),
+        pltpu.make_async_copy(down_ref, whole.at[mine, pl.ds(1664, 512)], own_sem.at[3]),
+        pltpu.make_async_copy(x_ref, x_all.at[tp], own_sem.at[4]),
     ]
     for one in own:
         one.start()
     for one in own:
         one.wait()
-    pl.semaphore_wait(barrier, 8)
+    pl.semaphore_wait(barrier, 7)
 
     def copy_of(m, step):
         o = dict(m["o"])
@@ -275,7 +289,7 @@
         return pltpu.make_async_remote_copy(
             src_ref=at,
             dst_ref=at,
-            send_sem=send_sem.at[m["id"]],
+            send_sem=send_sem.at[0],
             recv_sem=recv_sem.at[m["id"]],
             device_id=neighbour(m["axis"], m["sign"]),
             device_id_type=MESH,
@@ -291,8 +305,8 @@
     def pump(until):
         while at_message[0] < len(order) and order[at_message[0]]["start"] <= until:
             m = order[at_message[0]]
-            if m["dep"] is not None:
-                arrived(m["dep"])
+            for d in m["deps"]:
+                arrived(d)
             copy_of(m, 0).start()
             at_message[0] += 1
 
@@ -319,23 +333,40 @@
         copy.start()
         started.append(copy)
 
+    right, left = peer(1), peer(3)
+    low, high = pl.ds(0, LENGTH // 2), pl.ds(LENGTH // 2, LENGTH // 2)
+
+    def move(buf, owner, rows, number, to):
+        at = buf.at[owner, rows]
+        return tp_copy(at, at, number, to)
+
     def share(buf, base):
-        for d in (2, 1, 3):
-            begin(tp_copy(buf.at[tp], buf.at[tp], base + d - 1, peer(d)))
-        begin(tp_copy(buf.at[tp], buf.at[tp], base + 3, partner))
+        begin(move(buf, tp, low, base, right))
+        begin(move(buf, tp, high, base + 1, left))
+        begin(move(buf, tp, high, base + 2, right))
+        begin(move(buf, tp, low, base + 3, left))
+        begin(tp_copy(buf.at[tp], buf.at[tp], base + 6, partner))
 
     def share_on(buf, base):
-        for d in (1, 3, 2):
-            came = buf.at[peer(-d)]
-            tp_copy(came, came, base + d - 1, peer(d)).wait_recv()
-            begin(tp_copy(came, came, base + 3 + d, partner))
+        move(buf, left, low, base, right).wait_recv()
+        begin(move(buf, left, low, base + 4, right))
+        move(buf, right, high, base + 1, left).wait_recv()
+        begin(move(buf, right, high, base + 5, left))
+        move(buf, left, high, base + 2, right).wait_recv()
+        begin(tp_copy(buf.at[left], buf.at[left], base + 7, partner))
+        move(buf, right, low, base + 3, left).wait_recv()
+        begin(tp_copy(buf.at[right], buf.at[right], base + 8, partner))
 
     def shared(buf, base):
-        for d in range(4):
-            came = buf.at[lax.rem(chip + 4 - d, 4) * 2 + (1 - core)]
-            tp_copy(came, came, base + 3 + d, partner).wait_recv()
-
-    def summed(product, got, paired, chips, base, clock):
+        far = peer(2)
+        move(buf, far, low, base + 4, right).wait_recv()
+        move(buf, far, high, base + 5, left).wait_recv()
+        begin(tp_copy(buf.at[far], buf.at[far], base + 9, partner))
+        for k, d in enumerate((0, 3, 1, 2)):
+            came = buf.at[lax.rem(chip + d, 4) * 2 + (1 - core)]
+            tp_copy(came, came, base + 6 + k, partner).wait_recv()
+
+    def summed(product, got, paired, through, joined, chips, base, clock):
         waiting = []
         for d in (2, 1, 3, 0):
             there = lax.rem(chip + d, 4) * 2
@@ -344,36 +375,46 @@
             for copy in waiting:
                 begin(copy)
             waiting = [tp_copy(sums.at[there + 1 - core], got.at[d], base + d, partner)]
-            pump(clock(d))
         for copy in waiting:
             begin(copy)
-        waiting = []
         for d in (2, 1, 3):
             there = lax.rem(chip + d, 4) * 2 + core
             tp_copy(sums.at[there], got.at[d], base + d, partner).wait_recv()
             paired[d - 1] = (sums[there].astype(f32) + got[d].astype(f32)).astype(bf16)
-            for copy in waiting:
-                begin(copy)
-            waiting = [tp_copy(paired.at[d - 1], chips.at[d - 1], base + 3 + d, peer(d))]
+            if d == 1:
+                begin(tp_copy(paired.at[1, low], through.at[0], base + 4, right))
+                begin(tp_copy(paired.at[1, high], through.at[1], base + 5, left))
+            if d == 3:
+                begin(tp_copy(paired.at[0, high], chips.at[0, high], base + 6, right))
         tp_copy(sums.at[tp], got.at[0], base, partner).wait_recv()
-        for copy in waiting:
-            begin(copy)
         total = sums[tp].astype(f32) + got[0].astype(f32)
-        return total
-
-    def chips_added(total, chips, base):
-        for d in (1, 3, 2):
-            tp_copy(chips.at[d - 1], chips.at[d - 1], base + 3 + d, peer(d)).wait_recv()
-            total = total + chips[d - 1].astype(f32)
-        return total
-
-    last = order[-1]["start"]
+        begin(tp_copy(paired.at[2, low], chips.at[1, low], base + 7, left))
+        clock()
+        tp_copy(through.at[0], through.at[0], base + 4, right).wait_recv()
+        half = LENGTH // 2
+        joined[0] = (paired[0, 0:half].astype(f32) + through[0].astype(f32)).astype(bf16)
+        tp_copy(through.at[1], through.at[1], base + 5, left).wait_recv()
+        joined[1] = (paired[2, half:].astype(f32) + through[1].astype(f32)).astype(bf16)
+        begin(tp_copy(joined.at[0], chips.at[0, low], base + 8, right))
+        for copy in started[: len(started) - 9]:
+            if id(copy) not in sent:
+                sent.add(id(copy))
+                copy.wait_send()
+        begin(tp_copy(joined.at[1], chips.at[1, high], base + 9, left))
+        clock()
+        tp_copy(chips.at[0, high], chips.at[0, high], base + 6, right).wait_recv()
+        tp_copy(chips.at[1, low], chips.at[1, low], base + 7, left).wait_recv()
+        tp_copy(chips.at[0, low], chips.at[0, low], base + 8, right).wait_recv()
+        tp_copy(chips.at[1, high], chips.at[1, high], base + 9, left).wait_recv()
+        return total + chips[0].astype(f32) + chips[1].astype(f32)
+
+    sent = set()
     share(x_all, 0)
     pump(T_SHARE)
     share_on(x_all, 0)
     pump(T_SHARED)
     shared(x_all, 0)
-    rows_norm(x_all, pre_ref, normed)
+    rows_norm(x_all, gains_ref, 0, normed)
     now = class_arrived(0)
 
     first = jnp.dot(normed[...], whole[:, 0:256], preferred_element_type=f32)
@@ -402,19 +443,24 @@
             gated, whole[rows, 512:640], (((1,), (1,)), ((), ())), preferred_element_type=f32
         )
 
-    begun = now
-    total = summed(mix_part, from_partner, pair_sums, from_chips, 8, lambda d: begun + 2.0)
-    pump(begun + 5.0)
-    mix = chips_added(total, from_chips, 8).astype(bf16)
+    ticks = [now]
+
+    def tick(step):
+        ticks[0] = ticks[0] + step
+        pump(ticks[0])
+
+    total = summed(
+        mix_part, from_partner, pair_sums, passing, passed, from_chips, 10, lambda: tick(T_SUM)
+    )
+    mix = total.astype(bf16)
     mid_all[tp] = (x_all[tp].astype(f32) + mix.astype(f32)).astype(bf16)
-    pump(begun + 9.0)
-    share(mid_all, 16)
-    pump(begun + 12.0)
-    share_on(mid_all, 16)
-    pump(begun + 15.0)
-    shared(mid_all, 16)
-    rows_norm(mid_all, post_ref, normed)
-    pump(last)
+    tick(T_MID)
+    share(mid_all, 20)
+    tick(T_MID)
+    share_on(mid_all, 20)
+    tick(T_MID)
+    shared(mid_all, 20)
+    rows_norm(mid_all, gains_ref, 1, normed)
     class_arrived(1)
 
     for block in range(4):
@@ -438,21 +484,41 @@
             hidden[...], whole[rows, 1664:2176], (((1,), (1,)), ((), ())), preferred_element_type=f32
         )
 
-    for copy in started[7:14]:
-        copy.wait_send()
-    total = summed(down_part, down_from_partner, down_pair_sums, down_from_chips, 24, lambda d: last)
-    ffn = chips_added(total, down_from_chips, 24).astype(bf16)
-    out_ref[...] = (mid_all[tp].astype(f32) + ffn.astype(f32)).astype(bf16)
-
-    for copy in started[:7] + started[14:]:
-        copy.wait_send()
-    for m in order:
-        copy_of(m, 0).wait_send()
+    for copy in started:
+        if id(copy) not in sent:
+            sent.add(id(copy))
+            copy.wait_send()
+    total = summed(
+        down_part,
+        down_from_partner,
+        down_pair_sums,
+        down_passing,
+        down_passed,
+        down_from_chips,
+        30,
+        lambda: None,
+    )
+    out_ref[...] = (mid_all[tp].astype(f32) + total.astype(bf16).astype(f32)).astype(bf16)
+
+    for copy in started:
+        if id(copy) not in sent:
+            copy.wait_send()
+    rest = whole.at[pl.ds(0, 31 * ROWS)]
+    pltpu.make_async_remote_copy(
+        src_ref=rest,
+        dst_ref=rest,
+        send_sem=send_sem.at[0],
+        recv_sem=recv_sem.at[0],
+        device_id=neighbour("y", 1),
+        device_id_type=MESH,
+    ).wait_send()
 
 
 T_SHARE = 4.0
 T_SHARED = 9.0
 T_PIECE = 0.7
+T_SUM = 2.0
+T_MID = 2.5
 
 
 def shards(
@@ -483,13 +549,10 @@
             forgetting_matrix,
             jnp.zeros_like(forgetting_matrix),
             attend_result_matrix.T,
-            content_expand_matrix,
-            switch_expand_matrix,
-            contract_matrix.T,
         ),
         axis=1,
     )
-    order = plan(PARTS, rate=42e3, lat=2.5)
+    order = plan(PARTS, 44e3, 2.3, 0.07)
     count = len(order)
     block = (LENGTH, COLS)
     dma = pltpu.SemaphoreType.DMA
@@ -499,7 +562,7 @@
     return pl.pallas_call(
         functools.partial(layer_kernel, order),
         out_shape=jax.ShapeDtypeStruct(block, bf16),
-        in_specs=[hbm, hbm] + [vmem] * 7,
+        in_specs=[hbm] * 5 + [vmem] * 6,
         out_specs=vmem,
         scratch_shapes=[
             pltpu.VMEM((32 * ROWS, WIDTH), bf16),
@@ -508,29 +571,35 @@
             pltpu.VMEM((GROUP, *block), bf16),
             pltpu.VMEM((4, *block), bf16),
             pltpu.VMEM((3, *block), bf16),
-            pltpu.VMEM((3, *block), bf16),
+            pltpu.VMEM((2, LENGTH // 2, COLS), bf16),
+            pltpu.VMEM((2, LENGTH // 2, COLS), bf16),
+            pltpu.VMEM((2, *block), bf16),
             pltpu.VMEM((4, *block), bf16),
             pltpu.VMEM((3, *block), bf16),
-            pltpu.VMEM((3, *block), bf16),
+            pltpu.VMEM((2, LENGTH // 2, COLS), bf16),
+            pltpu.VMEM((2, LENGTH // 2, COLS), bf16),
+            pltpu.VMEM((2, *block), bf16),
             pltpu.VMEM((LENGTH, GROUP * COLS), bf16),
             pltpu.VMEM((LENGTH, 512), bf16),
-            dma((2,)),
+            dma((5,)),
+            dma((1,)),
             dma((count,)),
-            dma((count,)),
-            dma((32,)),
-            dma((32,)),
+            dma((40,)),
+            dma((40,)),
         ],
         compiler_params=pltpu.CompilerParams(
             collective_id=0, has_side_effects=True, vmem_limit_bytes=48 * 1024 * 1024
         ),
     )(
         packed,
+        content_expand_matrix,
+        switch_expand_matrix,
+        contract_matrix.T,
         incoming_features,
-        attend_prenormal_scale[None],
+        jnp.stack((attend_prenormal_scale, perceptron_scale)),
         forgetting_shift[None],
         spike_forget_logarithm,
         attend_unit_scale[None],
-        perceptron_scale[None],
         content_kernel,
         switch_kernel,
     )

time: 89.2 us -> 87.9 us (0.985)
  Pallas kernels: 84.8 us -> 83.5 us
    broadcast_in_dim x2 -> x0, local copies, waits for them, and re-layouts: 1.42 us -> none  [the longest x1 0.73 us: shards(): attend_prenormal_scale[None]]
    pallas_call x1, Pallas kernels: 84.8 us -> 83.5 us  [shards(): pl.pallas_call(functools.partial(layer_kernel, order), out_shape=jax.Shap...]
    unnamed x20 -> x30, local copies, waits for them, and re-layouts: 1.66 us -> 2.85 us
where the time goes in v2:
time: 87.9 us; the launch traced here: 87.5 us
  Pallas kernels  83.5 us (95%)
  local copies, waits for them, and re-layouts  3.8 us (4%)
    pallas_call x1, Pallas kernels, shards(): pl.pallas_call(functools.partial(layer_kernel, order), out_shape=jax.Shap...  83.5 us
    unnamed x30, local copies, waits for them, and re-layouts  2.85 us

profile of v2, /device:TPU:1, one launch (start us, length us, event | category | flops | bytes accessed | tf_op | source)
XLA Modules:
  0.0 87.5 jit_solution(7177284684873780617)
XLA Ops:
  0.0 0.7 copy-done.12
  0.7 0.0 copy-done.13
  0.7 0.0 copy-start.10
  0.7 0.0 copy-start.9
  0.8 0.0 copy-start.8
  0.8 0.6 copy-done.11
  1.4 0.0 copy-done.10
  1.4 0.0 copy-done.9
  1.5 0.0 copy-start.6
  1.5 0.0 copy-start.7
  1.5 0.9 %concatenate.3.packed_ref = bf16[64,640]{1,0:T(8,128)(2,1)S(1)} concatenate(bf16[64,64]{1,0:T(8,128)(2,1)S(1)} %copy-done.9, bf16[64,64]{1,0:T(8,128)(2,1)S(1)} %copy-done.10, bf16[64,128]{1,0:T(8,128)(2,1)S(1)} %copy-done.11, bf16[64,128]{1,0:T(8,128)(2,1)} %param.23, bf16[64,64]{1,0:T(8,128)(2,1)} %param.22, bf16[64,64]{1,0:T(8,128)(2,1)S(1)} %broadcast_in_dim.9, ...), dimensions={1} | concatenate | bytes 163840 | tf_op jit(solution)/shard_map/concatenate | solution.py:543
  2.4 0.0 copy-done.8
  2.4 0.0 copy-start
  2.5 0.0 copy-start.1
  2.5 0.1 copy.18.spike_ref
  2.6 0.0 copy-done.2
  2.6 0.0 copy-done.3
  2.6 0.0 copy-done.4
  2.6 0.0 copy-done.5
  2.6 0.0 copy-done.6
  2.6 0.7 copy-done
  3.3 0.0 copy-done.1
  3.3 83.5 %shard_map.163 = bf16[192,256]{1,0:T(8,128)(2,1)S(1)} custom-call(bf16[64,640]{1,0:T(8,128)(2,1)S(1)} %concatenate.3.packed_ref, bf16[64,512]{1,0:T(8,128)(2,1)S(1)} %copy-done.1, bf16[64,512]{1,0:T(8,128)(2,1)S(1)} %copy-done.2, bf16[64,512]{1,0:T(8,128)(2,1)S(1)} %bitcast.4, bf16[192,256]{1,0:T(8,128)(2,1)S(1)} %copy-done, ...), custom_call_target="tpu_custom_call" | custom-call | tf_op jit(solution)/shard_map/pallas_call | solution.py:562
  86.8 0.6 copy.20
  (12 shorter events, 0.1 us)
Async XLA Ops:
  0.0 0.7 copy-start.12
  0.0 0.7 copy-start.13
  0.7 0.7 copy-start.11
  0.7 0.7 copy-start.10
  0.7 0.7 copy-start.9
  0.8 1.7 %copy-start.8 = (f32[192,64]{0,1:T(8,128)S(1)}, f32[192,64]{0,1:T(8,128)}, u32[]{:S(2)}) copy-start(f32[192,64]{0,1:T(8,128)} %param.25) | copy-start | bytes 147460
  1.5 1.1 %copy-start.2 = (bf16[64,512]{1,0:T(8,128)(2,1)S(1)}, bf16[64,512]{1,0:T(8,128)(2,1)}, u32[]{:S(2)}) copy-start(bf16[64,512]{1,0:T(8,128)(2,1)} %gate_ref.1) | copy-start | bytes 196612
  1.5 1.1 %copy-start.3 = (bf16[512,64]{0,1:T(8,128)(2,1)S(1)}, bf16[512,64]{0,1:T(8,128)(2,1)}, u32[]{:S(2)}) copy-start(bf16[512,64]{0,1:T(8,128)(2,1)} %param.33) | copy-start | bytes 196612
  1.5 1.1 %copy-start.4 = (bf16[3,512]{1,0:T(4,128)(2,1)S(1)}, bf16[3,512]{1,0:T(4,128)(2,1)}, u32[]{:S(2)}) copy-start(bf16[3,512]{1,0:T(4,128)(2,1)} %value_taps.1) | copy-start | bytes 9220
  1.5 1.1 %copy-start.5 = (bf16[3,512]{1,0:T(4,128)(2,1)S(1)}, bf16[3,512]{1,0:T(4,128)(2,1)}, u32[]{:S(2)}) copy-start(bf16[3,512]{1,0:T(4,128)(2,1)} %gate_taps.1) | copy-start | bytes 9220
  1.5 1.1 %copy-start.6 = (f32[64]{0:T(128)S(1)}, f32[64]{0:T(128)}, u32[]{:S(2)}) copy-start(f32[64]{0:T(128)} %param.24) | copy-start | bytes 772
  1.5 1.1 %copy-start.7 = (bf16[128]{0:T(256)(128)(2,1)S(1)}, bf16[128]{0:T(256)(128)(2,1)}, u32[]{:S(2)}) copy-start(bf16[128]{0:T(256)(128)(2,1)} %param.26) | copy-start | bytes 772
  2.4 0.9 %copy-start = (bf16[192,256]{1,0:T(8,128)(2,1)S(1)}, bf16[192,256]{1,0:T(8,128)(2,1)}, u32[]{:S(2)}) copy-start(bf16[192,256]{1,0:T(8,128)(2,1)} %x_ref.1) | copy-start | bytes 294916
  2.5 0.9 %copy-start.1 = (bf16[64,512]{1,0:T(8,128)(2,1)S(1)}, bf16[64,512]{1,0:T(8,128)(2,1)}, u32[]{:S(2)}) copy-start(bf16[64,512]{1,0:T(8,128)(2,1)} %value_ref.1) | copy-start | bytes 196612

commit v3 on v2

--- a/solution.py
+++ b/solution.py
@@ -83,6 +83,18 @@
             depth[m["id"]] = 1 + max((depth_of(k) for k in kids.get(m["id"], ())), default=0)
         return depth[m["id"]]
 
+    groups = {}
+    for m in msgs:
+        m["dz"] = m["o"]["z"] + (m["sign"] if m["axis"] == "z" else 0)
+        m["dz"] = 4 if abs(m["dz"]) == 4 else m["dz"]
+        leaf = not kids.get(m["id"])
+        key = (m["lo"], m["axis"], m["dz"]) if leaf else m["id"]
+        groups.setdefault(key, []).append(m)
+    for i, members in enumerate(groups.values()):
+        for m in members:
+            m["sem"] = i
+            shared = not kids.get(m["id"])
+            m["leaves"] = sum(k["rn"] for k in members) if shared else None
     free = {(a, s): 0.0 for a in "yz" for s in (1, -1)}
     avail = {k: [] for k in free}
     events = [(0.0, 0, m["id"]) for m in msgs if not m["deps"]]
@@ -107,6 +119,10 @@
                     k["need"] -= 1
                     if k["need"] == 0:
                         heapq.heappush(events, (m["arrive"], 0, k["id"]))
+    for members in groups.values():
+        last = max(members, key=lambda m: m["arrive"])
+        for m in members:
+            m["final"] = m is last
     return order
 
 
@@ -195,7 +211,7 @@
     yield out.astype(jnp.bfloat16)
 
 
-def rows_norm(blocks, gain_ref, which, out):
+def rows_norm(blocks, gain_ref, out):
     total = jnp.zeros((LENGTH, COLS), jnp.float32)
     for t in range(GROUP):
         one = blocks[t].astype(jnp.float32)
@@ -204,7 +220,7 @@
     scale = lax.rsqrt(mean + norm_eps)
     for t in range(GROUP):
         at = slice(t * COLS, (t + 1) * COLS)
-        gain = gain_ref[which : which + 1, at].astype(jnp.float32)
+        gain = gain_ref[at].astype(jnp.float32).reshape(1, COLS)
         out[:, at] = (blocks[t].astype(jnp.float32) * scale * gain).astype(jnp.bfloat16)
 
 
@@ -217,17 +233,23 @@
 
 def layer_kernel(
     order,
-    packed_ref,
+    query_ref,
+    key_ref,
+    content_ref,
+    switch_ref,
+    forget_ref,
+    mix_ref,
     value_ref,
     gate_ref,
     down_ref,
     x_ref,
-    gains_ref,
+    pre_ref,
+    post_ref,
     shift_ref,
     spike_ref,
     unit_ref,
-    value_taps,
-    gate_taps,
+    value_taps_ref,
+    gate_taps_ref,
     out_ref,
     whole,
     x_all,
@@ -243,8 +265,18 @@
     down_passing,
     down_passed,
     down_from_chips,
+    down_sums,
     normed,
     hidden,
+    raised,
+    narrow,
+    pre_gain,
+    post_gain,
+    shift_row,
+    spike_turned,
+    unit_row,
+    value_taps,
+    gate_taps,
     own_sem,
     send_sem,
     recv_sem,
@@ -268,16 +300,33 @@
     for other in (peer(1), peer(3), partner):
         pl.semaphore_signal(barrier, inc=1, device_id={"tp": other}, device_id_type=MESH)
     mine = pl.ds(pl.multiple_of(lax.axis_index("fs") * ROWS, ROWS), ROWS)
-    own = [
-        pltpu.make_async_copy(packed_ref, whole.at[mine, pl.ds(0, 640)], own_sem.at[0]),
-        pltpu.make_async_copy(value_ref, whole.at[mine, pl.ds(640, 512)], own_sem.at[1]),
-        pltpu.make_async_copy(gate_ref, whole.at[mine, pl.ds(1152, 512)], own_sem.at[2]),
-        pltpu.make_async_copy(down_ref, whole.at[mine, pl.ds(1664, 512)], own_sem.at[3]),
-        pltpu.make_async_copy(x_ref, x_all.at[tp], own_sem.at[4]),
-    ]
+    pairs = (
+        (query_ref, narrow.at[0]),
+        (key_ref, narrow.at[1]),
+        (forget_ref, narrow.at[2]),
+        (content_ref, whole.at[mine, pl.ds(128, 128)]),
+        (switch_ref, whole.at[mine, pl.ds(256, 128)]),
+        (mix_ref, whole.at[mine, pl.ds(512, 128)]),
+        (value_ref, whole.at[mine, pl.ds(640, 512)]),
+        (gate_ref, whole.at[mine, pl.ds(1152, 512)]),
+        (down_ref, whole.at[mine, pl.ds(1664, 512)]),
+        (x_ref, x_all.at[tp]),
+        (pre_ref, pre_gain),
+        (post_ref, post_gain),
+        (shift_ref, shift_row),
+        (spike_ref, spike_turned),
+        (unit_ref, unit_row),
+        (value_taps_ref, value_taps),
+        (gate_taps_ref, gate_taps),
+    )
+    own = [pltpu.make_async_copy(a, b, own_sem.at[i]) for i, (a, b) in enumerate(pairs)]
     for one in own:
         one.start()
-    for one in own:
+    for one in own[:3]:
+        one.wait()
+    whole[mine, 0:128] = jnp.concatenate((narrow[0], narrow[1]), axis=1)
+    whole[mine, 384:512] = jnp.concatenate((narrow[2], jnp.zeros_like(narrow[2])), axis=1)
+    for one in own[3:]:
         one.wait()
     pl.semaphore_wait(barrier, 7)
 
@@ -290,7 +339,7 @@
             src_ref=at,
             dst_ref=at,
             send_sem=send_sem.at[0],
-            recv_sem=recv_sem.at[m["id"]],
+            recv_sem=recv_sem.at[m["sem"]],
             device_id=neighbour(m["axis"], m["sign"]),
             device_id_type=MESH,
         )
@@ -298,9 +347,20 @@
     seen, at_message = set(), [0]
 
     def arrived(m):
-        if m["id"] not in seen:
-            copy_of(m, 1).wait_recv()
-            seen.add(m["id"])
+        if m["sem"] not in seen:
+            seen.add(m["sem"])
+            if m["leaves"] is None:
+                copy_of(m, 1).wait_recv()
+                return
+            at = whole.at[pl.ds(0, m["leaves"]), pl.ds(m["lo"], m["hi"] - m["lo"])]
+            pltpu.make_async_remote_copy(
+                src_ref=at,
+                dst_ref=at,
+                send_sem=send_sem.at[0],
+                recv_sem=recv_sem.at[m["sem"]],
+                device_id=neighbour(m["axis"], m["sign"]),
+                device_id_type=MESH,
+            ).wait_recv()
 
     def pump(until):
         while at_message[0] < len(order) and order[at_message[0]]["start"] <= until:
@@ -313,25 +373,30 @@
     def class_arrived(cls):
         mine_of = sorted((m for m in order if m["cls"] == cls), key=lambda m: m["arrive"])
         for m in mine_of:
-            pump(m["arrive"])
-            arrived(m)
+            if m["leaves"] is None or m["final"]:
+                pump(m["arrive"])
+                arrived(m)
         return mine_of[-1]["arrive"]
+
+    def from_depth(cls, dz):
+        came = [m for m in order if m["cls"] == cls and m["dz"] == dz]
+        for m in sorted(came, key=lambda m: m["arrive"]):
+            if m["leaves"] is None or m["final"]:
+                pump(m["arrive"])
+                arrived(m)
 
     def tp_copy(src, dst, number, to):
         return pltpu.make_async_remote_copy(
             src_ref=src,
             dst_ref=dst,
-            send_sem=tp_send.at[number],
+            send_sem=tp_send.at[number // 10],
             recv_sem=tp_recv.at[number],
             device_id={"tp": to},
             device_id_type=MESH,
         )
 
-    started = []
-
     def begin(copy):
         copy.start()
-        started.append(copy)
 
     right, left = peer(1), peer(3)
     low, high = pl.ds(0, LENGTH // 2), pl.ds(LENGTH // 2, LENGTH // 2)
@@ -366,26 +431,34 @@
             came = buf.at[lax.rem(chip + d, 4) * 2 + (1 - core)]
             tp_copy(came, came, base + 6 + k, partner).wait_recv()
 
-    def summed(product, got, paired, through, joined, chips, base, clock):
-        waiting = []
-        for d in (2, 1, 3, 0):
+    def summed(product, sums, got, paired, through, joined, chips, base, clock):
+        def products(d, before):
             there = lax.rem(chip + d, 4) * 2
-            for who in (1 - core, core):
-                sums[there + who] = product(there + who).astype(bf16)
-            for copy in waiting:
-                begin(copy)
-            waiting = [tp_copy(sums.at[there + 1 - core], got.at[d], base + d, partner)]
-        for copy in waiting:
-            begin(copy)
-        for d in (2, 1, 3):
+            sums[there + 1 - core] = product(there + 1 - core).astype(bf16)
+            if before is not None:
+                begin(before)
+            sums[there + core] = product(there + core).astype(bf16)
+            return tp_copy(sums.at[there + 1 - core], got.at[d], base + d, partner)
+
+        def pair(d):
             there = lax.rem(chip + d, 4) * 2 + core
             tp_copy(sums.at[there], got.at[d], base + d, partner).wait_recv()
             paired[d - 1] = (sums[there].astype(f32) + got[d].astype(f32)).astype(bf16)
-            if d == 1:
-                begin(tp_copy(paired.at[1, low], through.at[0], base + 4, right))
-                begin(tp_copy(paired.at[1, high], through.at[1], base + 5, left))
-            if d == 3:
-                begin(tp_copy(paired.at[0, high], chips.at[0, high], base + 6, right))
+
+        ready = products(2, None)
+        begin(ready)
+        ready = products(1, None)
+        begin(ready)
+        ready = products(3, None)
+        begin(ready)
+        pair(2)
+        ready = products(0, None)
+        begin(tp_copy(paired.at[1, low], through.at[0], base + 4, right))
+        begin(tp_copy(paired.at[1, high], through.at[1], base + 5, left))
+        begin(ready)
+        pair(1)
+        pair(3)
+        begin(tp_copy(paired.at[0, high], chips.at[0, high], base + 6, right))
         tp_copy(sums.at[tp], got.at[0], base, partner).wait_recv()
         total = sums[tp].astype(f32) + got[0].astype(f32)
         begin(tp_copy(paired.at[2, low], chips.at[1, low], base + 7, left))
@@ -396,10 +469,6 @@
         tp_copy(through.at[1], through.at[1], base + 5, left).wait_recv()
         joined[1] = (paired[2, half:].astype(f32) + through[1].astype(f32)).astype(bf16)
         begin(tp_copy(joined.at[0], chips.at[0, low], base + 8, right))
-        for copy in started[: len(started) - 9]:
-            if id(copy) not in sent:
-                sent.add(id(copy))
-                copy.wait_send()
         begin(tp_copy(joined.at[1], chips.at[1, high], base + 9, left))
         clock()
         tp_copy(chips.at[0, high], chips.at[0, high], base + 6, right).wait_recv()
@@ -408,13 +477,12 @@
         tp_copy(chips.at[1, high], chips.at[1, high], base + 9, left).wait_recv()
         return total + chips[0].astype(f32) + chips[1].astype(f32)
 
-    sent = set()
     share(x_all, 0)
     pump(T_SHARE)
     share_on(x_all, 0)
     pump(T_SHARED)
     shared(x_all, 0)
-    rows_norm(x_all, gains_ref, 0, normed)
+    rows_norm(x_all, pre_gain, normed)
     now = class_arrived(0)
 
     first = jnp.dot(normed[...], whole[:, 0:256], preferred_element_type=f32)
@@ -425,10 +493,10 @@
     key = rounded[:, 64:128]
     value = rounded[:, 128:256]
     gate = second[:, 0:128].astype(bf16).astype(f32)
-    forget = second[:, 128:192] + shift_ref[...]
+    forget = second[:, 128:192] + shift_row[...]
     decay = -(jnp.maximum(-forget, 0.0) + jnp.log1p(jnp.exp(-jnp.abs(forget)))) / 16.0
-    decay = decay + spike_ref[...]
-    unit = unit_ref[...].astype(f32)
+    decay = decay + spike_turned[...].T
+    unit = unit_row[...].astype(f32)
     now = now + 2.0
     for piece in attention_pieces(
         query, key, value, gate, decay, unit, lambda a, s: pltpu.roll(a, s, 0)
@@ -450,7 +518,7 @@
         pump(ticks[0])
 
     total = summed(
-        mix_part, from_partner, pair_sums, passing, passed, from_chips, 10, lambda: tick(T_SUM)
+        mix_part, sums, from_partner, pair_sums, passing, passed, from_chips, 10, lambda: tick(T_SUM)
     )
     mix = total.astype(bf16)
     mid_all[tp] = (x_all[tp].astype(f32) + mix.astype(f32)).astype(bf16)
@@ -460,18 +528,27 @@
     share_on(mid_all, 20)
     tick(T_MID)
     shared(mid_all, 20)
-    rows_norm(mid_all, gains_ref, 1, normed)
+    rows_norm(mid_all, post_gain, normed)
+    for dz in (0, 1, -1, 2, -2, 3, -3, 4):
+        from_depth(1, dz)
+        z = lax.rem(lax.axis_index("fs") // 4 + 16 - dz, 8)
+        deep = pl.ds(pl.multiple_of(z * 256, 256), 256)
+        for at in (0, 512):
+            part = jnp.dot(
+                normed[:, deep], whole[deep, 640 + at : 1152 + at], preferred_element_type=f32
+            )
+            if dz == 0:
+                raised[:, at : at + 512] = part
+            else:
+                raised[:, at : at + 512] = raised[:, at : at + 512] + part
     class_arrived(1)
+    pump(1e9)
 
     for block in range(4):
         at = block * 128
         cols = slice(at, at + 128)
-        up_value = jnp.dot(
-            normed[...], whole[:, 640 + at : 768 + at], preferred_element_type=f32
-        )
-        up_gate = jnp.dot(
-            normed[...], whole[:, 1152 + at : 1280 + at], preferred_element_type=f32
-        )
+        up_value = raised[:, at : at + 128]
+        up_gate = raised[:, 512 + at : 640 + at]
         conv_value = short_conv(up_value.astype(bf16).astype(f32), value_taps[:, cols].astype(f32))
         conv_gate = short_conv(up_gate.astype(bf16).astype(f32), gate_taps[:, cols].astype(f32))
         cube = conv_gate + 0.044715 * (conv_gate * conv_gate * conv_gate)
@@ -484,12 +561,9 @@
             hidden[...], whole[rows, 1664:2176], (((1,), (1,)), ((), ())), preferred_element_type=f32
         )
 
-    for copy in started:
-        if id(copy) not in sent:
-            sent.add(id(copy))
-            copy.wait_send()
     total = summed(
         down_part,
+        down_sums,
         down_from_partner,
         down_pair_sums,
         down_passing,
@@ -500,9 +574,9 @@
     )
     out_ref[...] = (mid_all[tp].astype(f32) + total.astype(bf16).astype(f32)).astype(bf16)
 
-    for copy in started:
-        if id(copy) not in sent:
-            copy.wait_send()
+    seven = x_all.at[pl.ds(0, 7)]
+    for group in range(4):
+        tp_copy(seven, seven, group * 10, partner).wait_send()
     rest = whole.at[pl.ds(0, 31 * ROWS)]
     pltpu.make_async_remote_copy(
         src_ref=rest,
@@ -540,20 +614,8 @@
     switch_kernel,
     contract_matrix,
 ):
-    packed = jnp.concatenate(
-        (
-            probe_matrix,
-            lookup_matrix,
-            content_matrix,
-            result_switch_matrix,
-            forgetting_matrix,
-            jnp.zeros_like(forgetting_matrix),
-            attend_result_matrix.T,
-        ),
-        axis=1,
-    )
     order = plan(PARTS, 44e3, 2.3, 0.07)
-    count = len(order)
+    count = 1 + max(m["sem"] for m in order)
     block = (LENGTH, COLS)
     dma = pltpu.SemaphoreType.DMA
     vmem = pl.BlockSpec(memory_space=pltpu.VMEM)
@@ -562,7 +624,7 @@
     return pl.pallas_call(
         functools.partial(layer_kernel, order),
         out_shape=jax.ShapeDtypeStruct(block, bf16),
-        in_specs=[hbm] * 5 + [vmem] * 6,
+        in_specs=[hbm] * 17,
         out_specs=vmem,
         scratch_shapes=[
             pltpu.VMEM((32 * ROWS, WIDTH), bf16),
@@ -579,26 +641,42 @@
             pltpu.VMEM((2, LENGTH // 2, COLS), bf16),
             pltpu.VMEM((2, LENGTH // 2, COLS), bf16),
             pltpu.VMEM((2, *block), bf16),
+            pltpu.VMEM((GROUP, *block), bf16),
             pltpu.VMEM((LENGTH, GROUP * COLS), bf16),
             pltpu.VMEM((LENGTH, 512), bf16),
-            dma((5,)),
+            pltpu.VMEM((LENGTH, 1024), jnp.float32),
+            pltpu.VMEM((3, ROWS, 64), bf16),
+            pltpu.VMEM((2048,), bf16),
+            pltpu.VMEM((2048,), bf16),
+            pltpu.VMEM((1, 64), jnp.float32),
+            pltpu.VMEM((64, LENGTH), jnp.float32),
+            pltpu.VMEM((1, 128), bf16),
+            pltpu.VMEM((3, 512), bf16),
+            pltpu.VMEM((3, 512), bf16),
+            dma((17,)),
             dma((1,)),
             dma((count,)),
-            dma((40,)),
+            dma((4,)),
             dma((40,)),
         ],
         compiler_params=pltpu.CompilerParams(
-            collective_id=0, has_side_effects=True, vmem_limit_bytes=48 * 1024 * 1024
+            collective_id=0, has_side_effects=True, vmem_limit_bytes=67043328
         ),
     )(
-        packed,
+        probe_matrix,
+        lookup_matrix,
+        content_matrix,
+        result_switch_matrix,
+        forgetting_matrix,
+        attend_result_matrix.T,
         content_expand_matrix,
         switch_expand_matrix,
         contract_matrix.T,
         incoming_features,
-        jnp.stack((attend_prenormal_scale, perceptron_scale)),
+        attend_prenormal_scale,
+        perceptron_scale,
         forgetting_shift[None],
-        spike_forget_logarithm,
+        spike_forget_logarithm.T,
         attend_unit_scale[None],
         content_kernel,
         switch_kernel,

time: 87.9 us -> 83.9 us (0.954)
  local copies, waits for them, and re-layouts: 3.8 us -> 1.54 us
  Pallas kernels: 83.5 us -> 81.5 us
    pallas_call x1, Pallas kernels: 83.5 us -> 81.5 us  [shards(): pl.pallas_call(functools.partial(layer_kernel, order), out_shape=jax.Shap...]
    unnamed x30 -> x1, local copies, waits for them, and re-layouts: 2.85 us -> 1.54 us
    concatenate x1 -> x0, local copies, waits for them, and re-layouts: 0.93 us -> none  [shards(): jnp.concatenate((probe_matrix, lookup_matrix, content_matrix, result_swit...]
where the time goes in v3:
time: 83.9 us; the launch traced here: 83 us
  Pallas kernels  81.5 us (97%)
  local copies, waits for them, and re-layouts  1.54 us (2%)
    pallas_call x1, Pallas kernels, shards(): pl.pallas_call(functools.partial(layer_kernel, order), out_shape=jax.Shap...  81.5 us

profile of v3, /device:TPU:1, one launch (start us, length us, event | category | flops | bytes accessed | tf_op | source)
XLA Modules:
  0.0 83.0 jit_solution(10759196229798078599)
XLA Ops:
  0.0 81.5 %shard_map.163 = bf16[192,256]{1,0:T(8,128)(2,1)} custom-call(bf16[64,64]{1,0:T(8,128)(2,1)} %query_ref.1, bf16[64,64]{1,0:T(8,128)(2,1)} %key_ref.1, bf16[64,128]{1,0:T(8,128)(2,1)} %content_ref.1, bf16[64,128]{1,0:T(8,128)(2,1)} %switch_ref.1, bf16[64,64]{1,0:T(8,128)(2,1)} %forget_ref.1, bf16[64,128]{1,0:T(8,128)(2,1)} %bitcast.7, ...), custom_call_target="tpu_custom_call" | custom-call | tf_op jit(solution)/shard_map/pallas_call | solution.py:624
  81.5 1.5 %copy.19 = bf16[192,256]{1,0:T(8,128)(2,1)} copy(bf16[192,256]{1,0:T(8,128)(2,1)} %shard_map.163) | data formatting | bytes 196608

commit v4 on v3

--- a/solution.py
+++ b/solution.py
@@ -70,8 +70,23 @@
     for p in parts:
         msgs += tree_messages(*p)
     kids = {}
+    parents = {id(d) for m in msgs for d in m["deps"]}
+    twins = {}
+    for m in msgs:
+        m["dz"] = m["o"]["z"] + (m["sign"] if m["axis"] == "z" else 0)
+        m["dz"] = 4 if abs(m["dz"]) == 4 else m["dz"]
+        across = m["o"]["y" if m["axis"] == "z" else "z"]
+        if id(m) in parents:
+            m["key"] = (m["lo"], m["axis"], across, abs(m["off"]))
+        else:
+            m["key"] = (m["lo"], m["axis"], m["dz"], "leaf")
+        twins.setdefault(m["key"], []).append(m)
+    for m in msgs:
+        keys = dict.fromkeys(d["key"] for d in m["deps"])
+        m["deps"] = tuple(t for k in keys for t in twins[k])
     for i, m in enumerate(msgs):
         m["id"] = i
+    for m in msgs:
         m["bytes"] = m["rn"] * (m["hi"] - m["lo"]) * 2
         m["need"] = len(m["deps"])
         for d in m["deps"]:
@@ -83,18 +98,10 @@
             depth[m["id"]] = 1 + max((depth_of(k) for k in kids.get(m["id"], ())), default=0)
         return depth[m["id"]]
 
-    groups = {}
-    for m in msgs:
-        m["dz"] = m["o"]["z"] + (m["sign"] if m["axis"] == "z" else 0)
-        m["dz"] = 4 if abs(m["dz"]) == 4 else m["dz"]
-        leaf = not kids.get(m["id"])
-        key = (m["lo"], m["axis"], m["dz"]) if leaf else m["id"]
-        groups.setdefault(key, []).append(m)
-    for i, members in enumerate(groups.values()):
+    for i, members in enumerate(twins.values()):
         for m in members:
             m["sem"] = i
-            shared = not kids.get(m["id"])
-            m["leaves"] = sum(k["rn"] for k in members) if shared else None
+            m["together"] = sum(k["rn"] for k in members)
     free = {(a, s): 0.0 for a in "yz" for s in (1, -1)}
     avail = {k: [] for k in free}
     events = [(0.0, 0, m["id"]) for m in msgs if not m["deps"]]
@@ -119,7 +126,7 @@
                     k["need"] -= 1
                     if k["need"] == 0:
                         heapq.heappush(events, (m["arrive"], 0, k["id"]))
-    for members in groups.values():
+    for members in twins.values():
         last = max(members, key=lambda m: m["arrive"])
         for m in members:
             m["final"] = m is last
@@ -301,32 +308,37 @@
         pl.semaphore_signal(barrier, inc=1, device_id={"tp": other}, device_id_type=MESH)
     mine = pl.ds(pl.multiple_of(lax.axis_index("fs") * ROWS, ROWS), ROWS)
     pairs = (
-        (query_ref, narrow.at[0]),
-        (key_ref, narrow.at[1]),
-        (forget_ref, narrow.at[2]),
-        (content_ref, whole.at[mine, pl.ds(128, 128)]),
-        (switch_ref, whole.at[mine, pl.ds(256, 128)]),
-        (mix_ref, whole.at[mine, pl.ds(512, 128)]),
-        (value_ref, whole.at[mine, pl.ds(640, 512)]),
-        (gate_ref, whole.at[mine, pl.ds(1152, 512)]),
-        (down_ref, whole.at[mine, pl.ds(1664, 512)]),
-        (x_ref, x_all.at[tp]),
-        (pre_ref, pre_gain),
-        (post_ref, post_gain),
-        (shift_ref, shift_row),
-        (spike_ref, spike_turned),
-        (unit_ref, unit_row),
-        (value_taps_ref, value_taps),
-        (gate_taps_ref, gate_taps),
+        (query_ref, narrow.at[0], 0),
+        (key_ref, narrow.at[1], 0),
+        (forget_ref, narrow.at[2], 0),
+        (content_ref, whole.at[mine, pl.ds(128, 128)], 1),
+        (switch_ref, whole.at[mine, pl.ds(256, 128)], 1),
+        (mix_ref, whole.at[mine, pl.ds(512, 128)], 2),
+        (value_ref, whole.at[mine, pl.ds(640, 512)], 3),
+        (gate_ref, whole.at[mine, pl.ds(1152, 512)], 3),
+        (down_ref, whole.at[mine, pl.ds(1664, 512)], 3),
+        (x_ref, x_all.at[tp], 4),
+        (pre_ref, pre_gain, 5),
+        (post_ref, post_gain, 6),
+        (shift_ref, shift_row, 7),
+        (spike_ref, spike_turned, 8),
+        (unit_ref, unit_row, 9),
+        (value_taps_ref, value_taps, 10),
+        (gate_taps_ref, gate_taps, 11),
     )
-    own = [pltpu.make_async_copy(a, b, own_sem.at[i]) for i, (a, b) in enumerate(pairs)]
+    own = [pltpu.make_async_copy(a, b, own_sem.at[i]) for a, b, i in pairs]
     for one in own:
         one.start()
-    for one in own[:3]:
-        one.wait()
+
+    def landed(at, number):
+        pltpu.make_async_copy(at, at, own_sem.at[number]).wait()
+
+    landed(narrow, 0)
     whole[mine, 0:128] = jnp.concatenate((narrow[0], narrow[1]), axis=1)
     whole[mine, 384:512] = jnp.concatenate((narrow[2], jnp.zeros_like(narrow[2])), axis=1)
-    for one in own[3:]:
+    landed(whole.at[mine, pl.ds(128, 256)], 1)
+    landed(whole.at[mine, pl.ds(640, 1536)], 3)
+    for one in [own[5], *own[9:]]:
         one.wait()
     pl.semaphore_wait(barrier, 7)
 
@@ -349,10 +361,7 @@
     def arrived(m):
         if m["sem"] not in seen:
             seen.add(m["sem"])
-            if m["leaves"] is None:
-                copy_of(m, 1).wait_recv()
-                return
-            at = whole.at[pl.ds(0, m["leaves"]), pl.ds(m["lo"], m["hi"] - m["lo"])]
+            at = whole.at[pl.ds(0, m["together"]), pl.ds(m["lo"], m["hi"] - m["lo"])]
             pltpu.make_async_remote_copy(
                 src_ref=at,
                 dst_ref=at,
@@ -373,7 +382,7 @@
     def class_arrived(cls):
         mine_of = sorted((m for m in order if m["cls"] == cls), key=lambda m: m["arrive"])
         for m in mine_of:
-            if m["leaves"] is None or m["final"]:
+            if m["final"]:
                 pump(m["arrive"])
                 arrived(m)
         return mine_of[-1]["arrive"]
@@ -381,7 +390,7 @@
     def from_depth(cls, dz):
         came = [m for m in order if m["cls"] == cls and m["dz"] == dz]
         for m in sorted(came, key=lambda m: m["arrive"]):
-            if m["leaves"] is None or m["final"]:
+            if m["final"]:
                 pump(m["arrive"])
                 arrived(m)
 
@@ -405,38 +414,38 @@
         at = buf.at[owner, rows]
         return tp_copy(at, at, number, to)
 
-    def share(buf, base):
+    def share(buf, base, clock):
         begin(move(buf, tp, low, base, right))
         begin(move(buf, tp, high, base + 1, left))
         begin(move(buf, tp, high, base + 2, right))
         begin(move(buf, tp, low, base + 3, left))
         begin(tp_copy(buf.at[tp], buf.at[tp], base + 6, partner))
-
-    def share_on(buf, base):
+        clock(1.5)
+        clock(1.5)
         move(buf, left, low, base, right).wait_recv()
         begin(move(buf, left, low, base + 4, right))
         move(buf, right, high, base + 1, left).wait_recv()
         begin(move(buf, right, high, base + 5, left))
+        clock(1.0)
         move(buf, left, high, base + 2, right).wait_recv()
         begin(tp_copy(buf.at[left], buf.at[left], base + 7, partner))
         move(buf, right, low, base + 3, left).wait_recv()
         begin(tp_copy(buf.at[right], buf.at[right], base + 8, partner))
-
-    def shared(buf, base):
+        clock(1.0)
+        clock(1.0)
         far = peer(2)
         move(buf, far, low, base + 4, right).wait_recv()
         move(buf, far, high, base + 5, left).wait_recv()
         begin(tp_copy(buf.at[far], buf.at[far], base + 9, partner))
+        clock(1.0)
         for k, d in enumerate((0, 3, 1, 2)):
             came = buf.at[lax.rem(chip + d, 4) * 2 + (1 - core)]
             tp_copy(came, came, base + 6 + k, partner).wait_recv()
 
     def summed(product, sums, got, paired, through, joined, chips, base, clock):
-        def products(d, before):
+        def products(d):
             there = lax.rem(chip + d, 4) * 2
             sums[there + 1 - core] = product(there + 1 - core).astype(bf16)
-            if before is not None:
-                begin(before)
             sums[there + core] = product(there + core).astype(bf16)
             return tp_copy(sums.at[there + 1 - core], got.at[d], base + d, partner)
 
@@ -445,24 +454,24 @@
             tp_copy(sums.at[there], got.at[d], base + d, partner).wait_recv()
             paired[d - 1] = (sums[there].astype(f32) + got[d].astype(f32)).astype(bf16)
 
-        ready = products(2, None)
-        begin(ready)
-        ready = products(1, None)
-        begin(ready)
-        ready = products(3, None)
-        begin(ready)
+        for d in (2, 1, 3):
+            begin(products(d))
+            clock(0.25)
+        clock(0.5)
         pair(2)
-        ready = products(0, None)
+        ready = products(0)
         begin(tp_copy(paired.at[1, low], through.at[0], base + 4, right))
         begin(tp_copy(paired.at[1, high], through.at[1], base + 5, left))
         begin(ready)
+        clock(0.5)
         pair(1)
         pair(3)
         begin(tp_copy(paired.at[0, high], chips.at[0, high], base + 6, right))
         tp_copy(sums.at[tp], got.at[0], base, partner).wait_recv()
         total = sums[tp].astype(f32) + got[0].astype(f32)
         begin(tp_copy(paired.at[2, low], chips.at[1, low], base + 7, left))
-        clock()
+        clock(1.2)
+        clock(1.2)
         tp_copy(through.at[0], through.at[0], base + 4, right).wait_recv()
         half = LENGTH // 2
         joined[0] = (paired[0, 0:half].astype(f32) + through[0].astype(f32)).astype(bf16)
@@ -470,24 +479,30 @@
         joined[1] = (paired[2, half:].astype(f32) + through[1].astype(f32)).astype(bf16)
         begin(tp_copy(joined.at[0], chips.at[0, low], base + 8, right))
         begin(tp_copy(joined.at[1], chips.at[1, high], base + 9, left))
-        clock()
+        clock(1.3)
+        clock(1.3)
         tp_copy(chips.at[0, high], chips.at[0, high], base + 6, right).wait_recv()
         tp_copy(chips.at[1, low], chips.at[1, low], base + 7, left).wait_recv()
         tp_copy(chips.at[0, low], chips.at[0, low], base + 8, right).wait_recv()
         tp_copy(chips.at[1, high], chips.at[1, high], base + 9, left).wait_recv()
         return total + chips[0].astype(f32) + chips[1].astype(f32)
 
-    share(x_all, 0)
-    pump(T_SHARE)
-    share_on(x_all, 0)
-    pump(T_SHARED)
-    shared(x_all, 0)
+    ticks = [0.5]
+
+    def tick(step):
+        ticks[0] = ticks[0] + step
+        pump(ticks[0])
+
+    def still(step):
+        del step
+
+    share(x_all, 0, tick)
     rows_norm(x_all, pre_gain, normed)
-    now = class_arrived(0)
+    ticks[0] = class_arrived(0)
 
     first = jnp.dot(normed[...], whole[:, 0:256], preferred_element_type=f32)
     second = jnp.dot(normed[...], whole[:, 256:512], preferred_element_type=f32)
-    pump(now + 2.0)
+    tick(0.7)
     rounded = first.astype(bf16).astype(f32)
     query = rounded[:, 0:64] * HEAD_K ** (-0.5)
     key = rounded[:, 64:128]
@@ -497,12 +512,10 @@
     decay = -(jnp.maximum(-forget, 0.0) + jnp.log1p(jnp.exp(-jnp.abs(forget)))) / 16.0
     decay = decay + spike_turned[...].T
     unit = unit_row[...].astype(f32)
-    now = now + 2.0
     for piece in attention_pieces(
         query, key, value, gate, decay, unit, lambda a, s: pltpu.roll(a, s, 0)
     ):
-        now = now + T_PIECE
-        pump(now)
+        tick(T_PIECE)
         gated = piece
 
     def mix_part(t):
@@ -511,25 +524,19 @@
             gated, whole[rows, 512:640], (((1,), (1,)), ((), ())), preferred_element_type=f32
         )
 
-    ticks = [now]
-
-    def tick(step):
-        ticks[0] = ticks[0] + step
-        pump(ticks[0])
-
     total = summed(
-        mix_part, sums, from_partner, pair_sums, passing, passed, from_chips, 10, lambda: tick(T_SUM)
+        mix_part, sums, from_partner, pair_sums, passing, passed, from_chips, 10, tick
     )
     mix = total.astype(bf16)
     mid_all[tp] = (x_all[tp].astype(f32) + mix.astype(f32)).astype(bf16)
-    tick(T_MID)
-    share(mid_all, 20)
-    tick(T_MID)
-    share_on(mid_all, 20)
-    tick(T_MID)
-    shared(mid_all, 20)
+    share(mid_all, 20, tick)
     rows_norm(mid_all, post_gain, normed)
-    for dz in (0, 1, -1, 2, -2, 3, -3, 4):
+    last_of = {}
+    for m in order:
+        if m["cls"] == 1:
+            last_of[m["dz"]] = max(last_of.get(m["dz"], 0.0), m["arrive"])
+    by_arrival = sorted(last_of, key=last_of.get)
+    for dz in by_arrival:
         from_depth(1, dz)
         z = lax.rem(lax.axis_index("fs") // 4 + 16 - dz, 8)
         deep = pl.ds(pl.multiple_of(z * 256, 256), 256)
@@ -537,7 +544,7 @@
             part = jnp.dot(
                 normed[:, deep], whole[deep, 640 + at : 1152 + at], preferred_element_type=f32
             )
-            if dz == 0:
+            if dz == by_arrival[0]:
                 raised[:, at : at + 512] = part
             else:
                 raised[:, at : at + 512] = raised[:, at : at + 512] + part
@@ -570,7 +577,7 @@
         down_passed,
         down_from_chips,
         30,
-        lambda: None,
+        still,
     )
     out_ref[...] = (mid_all[tp].astype(f32) + total.astype(bf16).astype(f32)).astype(bf16)
 
@@ -588,11 +595,7 @@
     ).wait_send()
 
 
-T_SHARE = 4.0
-T_SHARED = 9.0
-T_PIECE = 0.7
-T_SUM = 2.0
-T_MID = 2.5
+T_PIECE = 0.55
 
 
 def shards(
@@ -614,12 +617,12 @@
     switch_kernel,
     contract_matrix,
 ):
-    order = plan(PARTS, 44e3, 2.3, 0.07)
+    order = plan(PARTS, 46.6e3, 1.8, 0.02)
     count = 1 + max(m["sem"] for m in order)
     block = (LENGTH, COLS)
     dma = pltpu.SemaphoreType.DMA
     vmem = pl.BlockSpec(memory_space=pltpu.VMEM)
-    hbm = pl.BlockSpec(memory_space=pl.ANY)
+    hbm = pl.BlockSpec(memory_space=pltpu.HBM)
     bf16 = jnp.bfloat16
     return pl.pallas_call(
         functools.partial(layer_kernel, order),
@@ -653,7 +656,7 @@
             pltpu.VMEM((1, 128), bf16),
             pltpu.VMEM((3, 512), bf16),
             pltpu.VMEM((3, 512), bf16),
-            dma((17,)),
+            dma((12,)),
             dma((1,)),
             dma((count,)),
             dma((4,)),

time: 83.9 us -> 84 us (level)
  no operation moved by 1% of the time
where the time goes in v4:
time: 84 us; the launch traced here: 83.8 us
  Pallas kernels  82.3 us (98%)
  local copies, waits for them, and re-layouts  1.54 us (2%)
    pallas_call x1, Pallas kernels, shards(): pl.pallas_call(functools.partial(layer_kernel, order), out_shape=jax.Shap...  82.3 us

profile of v4, /device:TPU:1, one launch (start us, length us, event | category | flops | bytes accessed | tf_op | source)
XLA Modules:
  0.0 83.8 jit_solution(13489185008216633498)
XLA Ops:
  0.0 82.3 %shard_map.163 = bf16[192,256]{1,0:T(8,128)(2,1)} custom-call(bf16[64,64]{1,0:T(8,128)(2,1)} %query_ref.1, bf16[64,64]{1,0:T(8,128)(2,1)} %key_ref.1, bf16[64,128]{1,0:T(8,128)(2,1)} %content_ref.1, bf16[64,128]{1,0:T(8,128)(2,1)} %switch_ref.1, bf16[64,64]{1,0:T(8,128)(2,1)} %forget_ref.1, bf16[64,128]{1,0:T(8,128)(2,1)} %bitcast.7, ...), custom_call_target="tpu_custom_call" | custom-call | tf_op jit(solution)/shard_map/pallas_call | solution.py:627
  82.3 1.5 %copy.19 = bf16[192,256]{1,0:T(8,128)(2,1)} copy(bf16[192,256]{1,0:T(8,128)(2,1)} %shard_map.163) | data formatting | bytes 196608

commit v5 on v4

--- a/solution.py
+++ b/solution.py
@@ -113,6 +113,7 @@
             _, kind, i = heapq.heappop(events)
             if kind == 0:
                 m = msgs[i]
+                m["ready"] = t
                 heapq.heappush(avail[(m["axis"], m["sign"])], (m["cls"], -depth_of(m), i))
         for link, queue in avail.items():
             if queue and free[link] <= t + 1e-9:
@@ -338,8 +339,8 @@
     whole[mine, 384:512] = jnp.concatenate((narrow[2], jnp.zeros_like(narrow[2])), axis=1)
     landed(whole.at[mine, pl.ds(128, 256)], 1)
     landed(whole.at[mine, pl.ds(640, 1536)], 3)
-    for one in [own[5], *own[9:]]:
-        one.wait()
+    own[5].wait()
+    own[9].wait()
     pl.semaphore_wait(barrier, 7)
 
     def copy_of(m, step):
@@ -356,7 +357,7 @@
             device_id_type=MESH,
         )
 
-    seen, at_message = set(), [0]
+    seen, waiting, ahead = set(), list(order), [AHEAD_FIRST]
 
     def arrived(m):
         if m["sem"] not in seen:
@@ -372,12 +373,15 @@
             ).wait_recv()
 
     def pump(until):
-        while at_message[0] < len(order) and order[at_message[0]]["start"] <= until:
-            m = order[at_message[0]]
+        later = []
+        for m in waiting:
+            if m["start"] > until + ahead[0] or m["ready"] > until:
+                later.append(m)
+                continue
             for d in m["deps"]:
                 arrived(d)
             copy_of(m, 0).start()
-            at_message[0] += 1
+        waiting[:] = later
 
     def class_arrived(cls):
         mine_of = sorted((m for m in order if m["cls"] == cls), key=lambda m: m["arrive"])
@@ -490,15 +494,19 @@
     ticks = [0.5]
 
     def tick(step):
-        ticks[0] = ticks[0] + step
+        ticks[0] = ticks[0] + PACE * step
         pump(ticks[0])
 
     def still(step):
         del step
 
     share(x_all, 0, tick)
+    for one in own[10:]:
+        one.wait()
     rows_norm(x_all, pre_gain, normed)
     ticks[0] = class_arrived(0)
+    ahead[0] = AHEAD
+    pump(ticks[0])
 
     first = jnp.dot(normed[...], whole[:, 0:256], preferred_element_type=f32)
     second = jnp.dot(normed[...], whole[:, 256:512], preferred_element_type=f32)
@@ -595,7 +603,10 @@
     ).wait_send()
 
 
-T_PIECE = 0.55
+T_PIECE = 0.5
+AHEAD_FIRST = 1.0
+AHEAD = 3.0
+PACE = 1.3
 
 
 def shards(

time: 84 us -> 77.5 us (0.923)
  Pallas kernels: 82.3 us -> 75.8 us
    pallas_call x1, Pallas kernels: 82.3 us -> 75.8 us  [shards(): pl.pallas_call(functools.partial(layer_kernel, order), out_shape=jax.Shap...]
where the time goes in v5:
time: 77.5 us; the launch traced here: 77.4 us
  Pallas kernels  75.8 us (98%)
  local copies, waits for them, and re-layouts  1.54 us (2%)
    pallas_call x1, Pallas kernels, shards(): pl.pallas_call(functools.partial(layer_kernel, order), out_shape=jax.Shap...  75.8 us

profile of v5, /device:TPU:1, one launch (start us, length us, event | category | flops | bytes accessed | tf_op | source)
XLA Modules:
  0.0 77.4 jit_solution(283222722716275175)
XLA Ops:
  0.0 75.8 %shard_map.163 = bf16[192,256]{1,0:T(8,128)(2,1)} custom-call(bf16[64,64]{1,0:T(8,128)(2,1)} %query_ref.1, bf16[64,64]{1,0:T(8,128)(2,1)} %key_ref.1, bf16[64,128]{1,0:T(8,128)(2,1)} %content_ref.1, bf16[64,128]{1,0:T(8,128)(2,1)} %switch_ref.1, bf16[64,64]{1,0:T(8,128)(2,1)} %forget_ref.1, bf16[64,128]{1,0:T(8,128)(2,1)} %bitcast.7, ...), custom_call_target="tpu_custom_call" | custom-call | tf_op jit(solution)/shard_map/pallas_call | solution.py:638
  75.8 1.5 %copy.19 = bf16[192,256]{1,0:T(8,128)(2,1)} copy(bf16[192,256]{1,0:T(8,128)(2,1)} %shard_map.163) | data formatting | bytes 196608

commit v6 on v5

--- a/solution.py
+++ b/solution.py
@@ -338,9 +338,7 @@
     whole[mine, 0:128] = jnp.concatenate((narrow[0], narrow[1]), axis=1)
     whole[mine, 384:512] = jnp.concatenate((narrow[2], jnp.zeros_like(narrow[2])), axis=1)
     landed(whole.at[mine, pl.ds(128, 256)], 1)
-    landed(whole.at[mine, pl.ds(640, 1536)], 3)
     own[5].wait()
-    own[9].wait()
     pl.semaphore_wait(barrier, 7)
 
     def copy_of(m, step):
@@ -403,7 +401,7 @@
             src_ref=src,
             dst_ref=dst,
             send_sem=tp_send.at[number // 10],
-            recv_sem=tp_recv.at[number],
+            recv_sem=tp_recv.at[number // 10 * 7 + number % 10],
             device_id={"tp": to},
             device_id_type=MESH,
         )
@@ -432,19 +430,18 @@
         begin(move(buf, right, high, base + 5, left))
         clock(1.0)
         move(buf, left, high, base + 2, right).wait_recv()
-        begin(tp_copy(buf.at[left], buf.at[left], base + 7, partner))
+        begin(tp_copy(buf.at[left], buf.at[left], base + 6, partner))
         move(buf, right, low, base + 3, left).wait_recv()
-        begin(tp_copy(buf.at[right], buf.at[right], base + 8, partner))
+        begin(tp_copy(buf.at[right], buf.at[right], base + 6, partner))
         clock(1.0)
         clock(1.0)
         far = peer(2)
         move(buf, far, low, base + 4, right).wait_recv()
         move(buf, far, high, base + 5, left).wait_recv()
-        begin(tp_copy(buf.at[far], buf.at[far], base + 9, partner))
+        begin(tp_copy(buf.at[far], buf.at[far], base + 6, partner))
         clock(1.0)
-        for k, d in enumerate((0, 3, 1, 2)):
-            came = buf.at[lax.rem(chip + d, 4) * 2 + (1 - core)]
-            tp_copy(came, came, base + 6 + k, partner).wait_recv()
+        came = buf.at[pl.ds(0, 4)]
+        tp_copy(came, came, base + 6, partner).wait_recv()
 
     def summed(product, sums, got, paired, through, joined, chips, base, clock):
         def products(d):
@@ -458,22 +455,20 @@
             tp_copy(sums.at[there], got.at[d], base + d, partner).wait_recv()
             paired[d - 1] = (sums[there].astype(f32) + got[d].astype(f32)).astype(bf16)
 
-        for d in (2, 1, 3):
+        for d in (2, 1, 3, 0):
             begin(products(d))
             clock(0.25)
-        clock(0.5)
+        clock(0.25)
         pair(2)
-        ready = products(0)
         begin(tp_copy(paired.at[1, low], through.at[0], base + 4, right))
         begin(tp_copy(paired.at[1, high], through.at[1], base + 5, left))
-        begin(ready)
         clock(0.5)
         pair(1)
         pair(3)
         begin(tp_copy(paired.at[0, high], chips.at[0, high], base + 6, right))
         tp_copy(sums.at[tp], got.at[0], base, partner).wait_recv()
         total = sums[tp].astype(f32) + got[0].astype(f32)
-        begin(tp_copy(paired.at[2, low], chips.at[1, low], base + 7, left))
+        begin(tp_copy(paired.at[2, low], chips.at[1, low], base + 6, left))
         clock(1.2)
         clock(1.2)
         tp_copy(through.at[0], through.at[0], base + 4, right).wait_recv()
@@ -481,14 +476,11 @@
         joined[0] = (paired[0, 0:half].astype(f32) + through[0].astype(f32)).astype(bf16)
         tp_copy(through.at[1], through.at[1], base + 5, left).wait_recv()
         joined[1] = (paired[2, half:].astype(f32) + through[1].astype(f32)).astype(bf16)
-        begin(tp_copy(joined.at[0], chips.at[0, low], base + 8, right))
-        begin(tp_copy(joined.at[1], chips.at[1, high], base + 9, left))
+        begin(tp_copy(joined.at[0], chips.at[0, low], base + 6, right))
+        begin(tp_copy(joined.at[1], chips.at[1, high], base + 6, left))
         clock(1.3)
         clock(1.3)
-        tp_copy(chips.at[0, high], chips.at[0, high], base + 6, right).wait_recv()
-        tp_copy(chips.at[1, low], chips.at[1, low], base + 7, left).wait_recv()
-        tp_copy(chips.at[0, low], chips.at[0, low], base + 8, right).wait_recv()
-        tp_copy(chips.at[1, high], chips.at[1, high], base + 9, left).wait_recv()
+        tp_copy(chips, chips, base + 6, right).wait_recv()
         return total + chips[0].astype(f32) + chips[1].astype(f32)
 
     ticks = [0.5]
@@ -500,6 +492,9 @@
     def still(step):
         del step
 
+    pump(0.0)
+    landed(whole.at[mine, pl.ds(640, 1536)], 3)
+    own[9].wait()
     share(x_all, 0, tick)
     for one in own[10:]:
         one.wait()
@@ -606,7 +601,7 @@
 T_PIECE = 0.5
 AHEAD_FIRST = 1.0
 AHEAD = 3.0
-PACE = 1.3
+PACE = 1.4
 
 
 def shards(
@@ -671,7 +666,7 @@
             dma((1,)),
             dma((count,)),
             dma((4,)),
-            dma((40,)),
+            dma((28,)),
         ],
         compiler_params=pltpu.CompilerParams(
             collective_id=0, has_side_effects=True, vmem_limit_bytes=67043328

time: 77.5 us -> 77 us (level)
  no operation moved by 1% of the time
where the time goes in v6:
time: 77 us; the launch traced here: 76.9 us
  Pallas kernels  75.3 us (98%)
  local copies, waits for them, and re-layouts  1.54 us (2%)
    pallas_call x1, Pallas kernels, shards(): pl.pallas_call(functools.partial(layer_kernel, order), out_shape=jax.Shap...  75.3 us
    unnamed x1, local copies, waits for them, and re-layouts  1.54 us

profile of v6, /device:TPU:1, one launch (start us, length us, event | category | flops | bytes accessed | tf_op | source)
XLA Modules:
  0.0 76.9 jit_solution(968780062669960299)
XLA Ops:
  0.0 75.3 %shard_map.163 = bf16[192,256]{1,0:T(8,128)(2,1)} custom-call(bf16[64,64]{1,0:T(8,128)(2,1)} %query_ref.1, bf16[64,64]{1,0:T(8,128)(2,1)} %key_ref.1, bf16[64,128]{1,0:T(8,128)(2,1)} %content_ref.1, bf16[64,128]{1,0:T(8,128)(2,1)} %switch_ref.1, bf16[64,64]{1,0:T(8,128)(2,1)} %forget_ref.1, bf16[64,128]{1,0:T(8,128)(2,1)} %bitcast.7, ...), custom_call_target="tpu_custom_call" | custom-call | tf_op jit(solution)/shard_map/pallas_call | solution.py:633
  75.3 1.5 %copy.19 = bf16[192,256]{1,0:T(8,128)(2,1)} copy(bf16[192,256]{1,0:T(8,128)(2,1)} %shard_map.163) | data formatting | bytes 196608

commit v7 on v6

--- a/solution.py
+++ b/solution.py
@@ -299,14 +299,6 @@
     def peer(d):
         return lax.rem(chip + 4 + d, 4) * 2 + core
 
-    barrier = pltpu.get_barrier_semaphore()
-    for axis in ("y", "z"):
-        for sign in (1, -1):
-            pl.semaphore_signal(
-                barrier, inc=1, device_id=neighbour(axis, sign), device_id_type=MESH
-            )
-    for other in (peer(1), peer(3), partner):
-        pl.semaphore_signal(barrier, inc=1, device_id={"tp": other}, device_id_type=MESH)
     mine = pl.ds(pl.multiple_of(lax.axis_index("fs") * ROWS, ROWS), ROWS)
     pairs = (
         (query_ref, narrow.at[0], 0),
@@ -328,7 +320,17 @@
         (gate_taps_ref, gate_taps, 11),
     )
     own = [pltpu.make_async_copy(a, b, own_sem.at[i]) for a, b, i in pairs]
-    for one in own:
+    for one in own[:10]:
+        one.start()
+    barrier = pltpu.get_barrier_semaphore()
+    for axis in ("y", "z"):
+        for sign in (1, -1):
+            pl.semaphore_signal(
+                barrier, inc=1, device_id=neighbour(axis, sign), device_id_type=MESH
+            )
+    for other in (peer(1), peer(3), partner):
+        pl.semaphore_signal(barrier, inc=1, device_id={"tp": other}, device_id_type=MESH)
+    for one in own[10:]:
         one.start()
 
     def landed(at, number):

time: 77 us -> 77.1 us (level)
  no operation moved by 1% of the time
where the time goes in v7:
time: 77.1 us; the launch traced here: 76.9 us
  Pallas kernels  75.3 us (98%)
  local copies, waits for them, and re-layouts  1.54 us (2%)
    pallas_call x1, Pallas kernels, shards(): pl.pallas_call(functools.partial(layer_kernel, order), out_shape=jax.Shap...  75.3 us

profile of v7, /device:TPU:1, one launch (start us, length us, event | category | flops | bytes accessed | tf_op | source)
XLA Modules:
  0.0 76.9 jit_solution(9958299022471482844)
XLA Ops:
  0.0 75.3 %shard_map.163 = bf16[192,256]{1,0:T(8,128)(2,1)} custom-call(bf16[64,64]{1,0:T(8,128)(2,1)} %query_ref.1, bf16[64,64]{1,0:T(8,128)(2,1)} %key_ref.1, bf16[64,128]{1,0:T(8,128)(2,1)} %content_ref.1, bf16[64,128]{1,0:T(8,128)(2,1)} %switch_ref.1, bf16[64,64]{1,0:T(8,128)(2,1)} %forget_ref.1, bf16[64,128]{1,0:T(8,128)(2,1)} %bitcast.7, ...), custom_call_target="tpu_custom_call" | custom-call | tf_op jit(solution)/shard_map/pallas_call | solution.py:635
  75.4 1.5 %copy.19 = bf16[192,256]{1,0:T(8,128)(2,1)} copy(bf16[192,256]{1,0:T(8,128)(2,1)} %shard_map.163) | data formatting | bytes 196608
